TPU v7x, 128 devices: a whole 4x4x4 slice. The times are simulated.
128 devices in a mesh: ep: 16 (over z, x), tp: 8 (over y, core).
Axes of the slice: x: 4, y: 4, z: 4, core: 2. Of those that a mesh axis runs over, the one named last changes fastest.
Arguments:
- residual: bfloat16 [2048, 2048], P('ep', 'tp'), may hold values from -61 to 61
- in_gain: float32 [2048], replicated, may hold values from 0.1 to 1.9
- in_weight: bfloat16 [2048, 1024], P(None, 'tp'), may hold values from -0.125 to 0.125
- state: float32 [2, 2048, 4096], P(None, 'ep', 'tp'), may hold values from -3 to 3
- decay_rate: float32 [64, 64], P('tp'), may hold values from 0.1 to 1
- frequency: float32 [64, 64], P('tp'), may hold values from 0 to 200
- log_step: float32 [64], P('tp'), may hold values from -3 to -0.7
- in_coef: float32 [2, 64, 64, 16], P(None, 'tp'), may hold values from -1 to 1
- out_coef: float32 [2, 64, 16, 64], P(None, 'tp'), may hold values from -0.75 to 0.75
- skip_gain: float32 [1024], P('tp'), may hold values from -3 to 3
- out_weight: bfloat16 [1024, 2048], replicated, may hold values from -0.1875 to 0.1875
- mid_gain: float32 [2048], replicated, may hold values from 0.1 to 1.9
- gate_vector: bfloat16 [2048], replicated, may hold values from -0.125 to 0.125
- routes: int32 [2048, 4], P('ep'), may hold values from 0 to 127, all different within a row; in each aligned block of 128 rows (0 to 127, 128 to 255, ...) at most 8 rows name the same one
- route_weight: float32 [2048, 4], P('ep'), may hold values from 0.1 to 1
- expert_gate: bfloat16 [128, 2048, 512], P(('ep', 'tp')), may hold values from -0.125 to 0.125
- expert_up: bfloat16 [128, 2048, 512], P(('ep', 'tp')), may hold values from -0.125 to 0.125
- expert_down: bfloat16 [128, 512, 2048], P(('ep', 'tp')), may hold values from -0.25 to 0.25
- shared_gate: bfloat16 [2048, 4096], P(None, 'ep'), may hold values from -0.125 to 0.125
- shared_up: bfloat16 [2048, 4096], P(None, 'ep'), may hold values from -0.125 to 0.125
- shared_down: bfloat16 [4096, 2048], P('ep'), may hold values from -0.09375 to 0.09375
Outputs:
- layer_out: bfloat16 [2048, 2048], P(('ep', 'tp'))
- new_state: float32 [2, 2048, 4096], P(None, 'ep', 'tp')
Inputs may be any that keep to these rules, and one draw needn't show every extreme that they name: `routes`: each row names 4 different experts. Among the rows of one index of ep no expert is named more than 8 times, a bound that some block reaches.
All inputs are finite; a program needn't handle non-finite values.
Results may differ from a plain program's by a relative error of at most 0.0085.
Values may be sent and summed in bfloat16 or wider, within the bound.
A program may use at most 128 MiB of HBM per device.

v0:
```python
import jax
import jax.numpy as jnp
from jax import lax
from jax.sharding import PartitionSpec as P

norm_eps = 1e-05
routed_scale = 2.5


def laid_out(blocks, dim):
    dims = list(blocks.shape[1:])
    dims[dim] *= blocks.shape[0]
    return jnp.moveaxis(blocks, 0, dim).reshape(dims)


def from_everyone(array, axis):
    length = lax.axis_size(axis)
    return lax.all_to_all(
        jnp.broadcast_to(array[None], (length, *array.shape)), axis, 0, 0, tiled=True
    )


def gather_directly(array, axis, dim):
    return laid_out(from_everyone(array, axis), dim)


def in_one_piece(arrays, axis, split_dim, concat_dim, along):
    both = jnp.concatenate(arrays, axis=along)
    result, at, finished = (
        lax.all_to_all(both, axis, split_axis=split_dim, concat_axis=concat_dim, tiled=True),
        0,
        [],
    )
    for a in arrays:
        finished.append(lax.slice_in_dim(result, at, at + a.shape[along], axis=along))
        at += a.shape[along]
    return tuple(finished)


def in_blocks(array, dim, length):
    before, after = (array.shape[:dim], array.shape[dim + 1 :])
    return jnp.moveaxis(array.reshape(*before, length, -1, *after), dim, 0)


def sent_and_summed(array, axis, dim):
    length = lax.axis_size(axis)
    blocks = lax.all_to_all(in_blocks(array, dim, length), axis, 0, 0, tiled=True)
    return jnp.sum(blocks.astype(jnp.float32), axis=0)


def layer_norm(values, gain_vec):
    row_mean = jnp.mean(values, axis=-1, keepdims=True)
    row_square = jnp.mean(values * values, axis=-1, keepdims=True)
    return (values - row_mean) * lax.rsqrt(row_square - row_mean * row_mean + norm_eps) * gain_vec


def coefficients(decay_rate, frequency, log_step, in_coef):
    time_step = jnp.exp(log_step)[:, None]
    real_rate = -decay_rate
    magnitude = jnp.exp(real_rate * time_step)
    keep_re = magnitude * jnp.cos(frequency * time_step)
    keep_im = magnitude * jnp.sin(frequency * time_step)
    denominator = real_rate * real_rate + frequency * frequency
    factor_re = ((keep_re - 1.0) * real_rate + keep_im * frequency) / denominator
    factor_im = (keep_im * real_rate - (keep_re - 1.0) * frequency) / denominator
    push_re = factor_re[..., None] * in_coef[0] - factor_im[..., None] * in_coef[1]
    push_im = factor_re[..., None] * in_coef[1] + factor_im[..., None] * in_coef[0]
    return (keep_re, keep_im, push_re, push_im)


def mixer_step(
    normed, in_weight, state, decay_rate, frequency, log_step, in_coef, out_coef, skip_gain
):
    row_count = normed.shape[0]
    group_count, state_count = decay_rate.shape
    keep_re, keep_im, push_re, push_im = coefficients(decay_rate, frequency, log_step, in_coef)
    drive = jnp.dot(normed, in_weight, preferred_element_type=jnp.float32).astype(jnp.bfloat16)
    drive_f = drive.astype(jnp.float32).reshape(row_count, group_count, -1)
    input_re = jnp.einsum("tgh,gph->tgp", drive_f, push_re)
    input_im = jnp.einsum("tgh,gph->tgp", drive_f, push_im)
    old_re = state[0].reshape(row_count, group_count, state_count)
    old_im = state[1].reshape(row_count, group_count, state_count)
    new_re = keep_re * old_re - keep_im * old_im + input_re
    new_im = keep_re * old_im + keep_im * old_re + input_im
    read_out = jnp.einsum("ghp,tgp->tgh", out_coef[0], new_re) - jnp.einsum(
        "ghp,tgp->tgh", out_coef[1], new_im
    )
    read_out = read_out.reshape(row_count, -1) + skip_gain * drive_f.reshape(row_count, -1)
    mixed_rows = jax.nn.gelu(read_out, approximate=True).astype(jnp.bfloat16)
    updated = jnp.stack([new_re.reshape(row_count, -1), new_im.reshape(row_count, -1)])
    return (mixed_rows, updated)


def route_slots(routes, experts):
    flat_routes = routes.reshape(-1)
    onehot = (flat_routes[:, None] == jnp.arange(experts, dtype=jnp.int32)[None, :]).astype(
        jnp.int32
    )
    before = jnp.cumsum(onehot, axis=0) - onehot
    return jnp.sum(before * onehot, axis=1).reshape(routes.shape)


def expert_block(row_block, gate_weight, up_weight, down_weight):
    gate_part = jnp.dot(row_block, gate_weight, preferred_element_type=jnp.float32)
    up_part = jnp.dot(row_block, up_weight, preferred_element_type=jnp.float32)
    hidden = (jax.nn.silu(gate_part) * up_part).astype(jnp.bfloat16)
    return jnp.dot(hidden, down_weight, preferred_element_type=jnp.float32).astype(jnp.bfloat16)


def per_device(
    residual,
    in_gain,
    in_weight,
    state,
    decay_rate,
    frequency,
    log_step,
    in_coef,
    out_coef,
    skip_gain,
    out_weight,
    mid_gain,
    gate_vector,
    routes,
    route_weight,
    expert_gate,
    expert_up,
    expert_down,
    shared_gate,
    shared_up,
    shared_down,
):
    tp_count = lax.axis_size("tp")
    ep_count = lax.axis_size("ep")
    tp_place = lax.axis_index("tp")
    seq_rows, feat_part = residual.shape
    width = feat_part * tp_count
    full_resid = gather_directly(residual, "tp", 1)
    normed = layer_norm(full_resid.astype(jnp.float32), in_gain).astype(jnp.bfloat16)
    mixed_part, new_state = mixer_step(
        normed, in_weight, state, decay_rate, frequency, log_step, in_coef, out_coef, skip_gain
    )
    mixed_rows = lax.all_gather(mixed_part, "tp", axis=1, tiled=True)
    after_mix = full_resid.astype(jnp.float32) + jnp.dot(
        mixed_rows, out_weight, preferred_element_type=jnp.float32
    )
    normed_mid = layer_norm(after_mix, mid_gain).astype(jnp.bfloat16)
    per_dev = seq_rows // tp_count
    own_mid = lax.dynamic_slice_in_dim(normed_mid, tp_place * per_dev, per_dev, 0)
    own_after = lax.dynamic_slice_in_dim(after_mix, tp_place * per_dev, per_dev, 0)
    experts = ep_count * tp_count
    top_count = routes.shape[1]
    capacity = max(2, 2 * seq_rows * top_count // experts)
    slot_rank = route_slots(routes, experts)
    dest_tp = routes % tp_count
    dest_ep = routes // tp_count
    is_mine = dest_tp == tp_place
    slot_place = dest_ep * capacity + slot_rank
    slot_total = ep_count * capacity
    matches = (
        slot_place.reshape(-1)[None, :] == jnp.arange(slot_total, dtype=jnp.int32)[:, None]
    ) & is_mine.reshape(-1)[None, :]
    token_ids = jnp.repeat(jnp.arange(seq_rows, dtype=jnp.int32), top_count)
    slot_token = jnp.sum(jnp.where(matches, token_ids[None, :], 0), axis=1)
    outgoing = normed_mid[slot_token].reshape(ep_count, capacity, width)
    copies = jnp.broadcast_to(own_mid[None], (ep_count, per_dev, width))
    got_slots, got_rows = in_one_piece((outgoing, copies), "ep", 0, 0, 1)
    flat_rows = got_slots.reshape(-1, width)
    result = expert_block(flat_rows, expert_gate[0], expert_up[0], expert_down[0])
    computed = result.reshape(got_slots.shape)
    returned = lax.all_to_all(computed, "ep", split_axis=0, concat_axis=0, tiled=True)
    piece = got_rows.reshape(-1, width)
    gate_part = jnp.dot(piece, shared_gate, preferred_element_type=jnp.float32)
    up_part = jnp.dot(piece, shared_up, preferred_element_type=jnp.float32)
    shared_hidden = (jax.nn.silu(gate_part) * up_part).astype(jnp.bfloat16)
    partial_rows = jnp.dot(shared_hidden, shared_down, preferred_element_type=jnp.float32)
    partial_back = lax.all_to_all(
        partial_rows.reshape(ep_count, per_dev, width).astype(jnp.bfloat16),
        "ep",
        split_axis=0,
        concat_axis=0,
        tiled=True,
    ).astype(jnp.float32)
    shared = jnp.sum(partial_back, axis=0)
    flat_back = returned.reshape(slot_total, width)
    weights = route_weight / jnp.sum(route_weight, axis=-1, keepdims=True) * routed_scale
    picked = flat_back[jnp.where(is_mine, slot_place, 0)].astype(jnp.float32)
    routed_part = jnp.sum(jnp.where(is_mine, weights, 0.0)[..., None] * picked, axis=1)
    routed = sent_and_summed(routed_part.astype(jnp.bfloat16), "tp", 0)
    gate_value = jax.nn.sigmoid(jnp.dot(own_mid, gate_vector, preferred_element_type=jnp.float32))
    layer_out = (own_after + routed + gate_value[:, None] * shared).astype(jnp.bfloat16)
    return (layer_out, new_state)


def solution(mesh):
    return jax.shard_map(
        per_device,
        mesh=mesh,
        in_specs=(
            P("ep", "tp"),
            P(),
            P(None, "tp"),
            P(None, "ep", "tp"),
            P("tp", None),
            P("tp", None),
            P("tp"),
            P(None, "tp", None, None),
            P(None, "tp", None, None),
            P("tp"),
            P(),
            P(),
            P(),
            P("ep", None),
            P("ep", None),
            P(("ep", "tp"), None, None),
            P(("ep", "tp"), None, None),
            P(("ep", "tp"), None, None),
            P(None, "ep"),
            P(None, "ep"),
            P("ep", None),
        ),
        out_specs=(P(("ep", "tp"), None), P(None, "ep", "tp")),
        check_vma=False,
    )
```

profile of v0, /device:TPU:0, one launch (start us, length us, event | category | flops | bytes accessed | tf_op | source)
XLA Modules:
  0.0 138.5 jit_solution(16512454888797237247)
XLA Ops:
  0.7 1.8 %broadcast_in_dim.22 = bf16[8,128,256]{2,1,0:T(8,128)(2,1)} broadcast(bf16[128,256]{1,0:T(8,128)(2,1)} %param.21), dimensions={1,2} | broadcast | bytes 589824 | tf_op jit(solution)/shard_map/broadcast_in_dim | solution.py:19
  2.5 4.6 %all-to-all-start = ((bf16[8,128,256]{2,1,0:T(8,128)(2,1)}), bf16[8,128,256]{2,1,0:T(8,128)(2,1)S(1)}, u32[]{:S(2)}, u32[]{:S(2)}) async-start(bf16[8,128,256]{2,1,0:T(8,128)(2,1)} %broadcast_in_dim.22), calls=%async_computation | async-start | bytes 1048576 | tf_op jit(solution)/shard_map/all_to_all | solution.py:18
  7.1 0.8 copy.88
  8.1 0.7 exp.17
  8.7 0.7 reduce_sum.94
  9.4 0.7 multiply_select_fusion
  11.6 1.1 fusion.78
  13.3 4.1 %all-to-all-done = bf16[8,128,256]{2,1,0:T(8,128)(2,1)S(1)} async-done(((bf16[8,128,256]{2,1,0:T(8,128)(2,1)}), bf16[8,128,256]{2,1,0:T(8,128)(2,1)S(1)}, u32[]{:S(2)}, u32[]{:S(2)}) %all-to-all-start) | async-done | bytes 524320 | tf_op jit(solution)/shard_map/all_to_all | solution.py:18
  19.9 12.8 %all_gather.3 = bf16[128,1024]{0,1:T(8,128)(2,1)S(1)} all-gather(bf16[128,128]{0,1:T(8,128)(2,1)S(1)} %fusion.50), channel_id=1, replica_groups=mesh['ep'=16,'tp'=8] {'tp'}, dimensions={1}, use_global_device_ids=true | all-gather | bytes 294912 | tf_op jit(solution)/shard_map/all_gather | solution.py:143
  32.7 0.8 fusion.75
  33.6 1.0 copy-done.2
  34.8 0.9 gather_fusion
  36.1 31.1 %all_to_all.25 = bf16[16,24,2048]{2,1,0:T(8,128)(2,1)S(1)} all-to-all(bf16[16,24,2048]{2,1,0:T(8,128)(2,1)S(1)} %pad_maximum_fusion), channel_id=1, replica_groups=mesh['ep'=16,'tp'=8] {'ep'}, dimensions={0} | all-to-all | bytes 3145728 | tf_op jit(solution)/shard_map/all_to_all | solution.py:30
  67.1 1.2 copy-done.1
  68.8 3.4 %fusion = bf16[16,8,2048]{2,1,0:T(8,128)(2,1)} fusion(bf16[1,512,2048]{2,1,0:T(8,128)(2,1)S(1)} %copy-done, bf16[1,2048,512]{2,1,0:T(8,128)(2,1)} %param.37, bf16[16,24,2048]{2,1,0:T(8,128)(2,1)} %copy-done.1, f32[128,512]{1,0:T(8,128)S(1)} %fusion.4), kind=kOutput, calls=%fused_computation.6 | convolution fusion | flops 537526272 | bytes 5505024 | tf_op jit(solution)/shard_map/dot_general | solution.py:107
  72.2 3.6 %all-to-all-start.2 = ((bf16[16,8,2048]{2,1,0:T(8,128)(2,1)}), bf16[16,8,2048]{2,1,0:T(8,128)(2,1)S(1)}, u32[]{:S(2)}, u32[]{:S(2)}) async-start(bf16[16,8,2048]{2,1,0:T(8,128)(2,1)} %fusion), calls=%async_computation.2 | async-start | bytes 1048576 | tf_op jit(solution)/shard_map/all_to_all | solution.py:171
  76.1 2.3 %slice.48 = bf16[16,16,2048]{2,1,0:T(8,128)(2,1)} slice(bf16[16,24,2048]{2,1,0:T(8,128)(2,1)} %copy-done.1), slice={[0:16], [8:24], [0:2048]} | slice | bytes 2097152 | tf_op jit(solution)/shard_map/slice | solution.py:35
  78.4 8.2 %all-to-all-done.2 = bf16[16,8,2048]{2,1,0:T(8,128)(2,1)S(1)} async-done(((bf16[16,8,2048]{2,1,0:T(8,128)(2,1)}), bf16[16,8,2048]{2,1,0:T(8,128)(2,1)S(1)}, u32[]{:S(2)}, u32[]{:S(2)}) %all-to-all-start.2) | async-done | bytes 524320 | tf_op jit(solution)/shard_map/all_to_all | solution.py:171
  86.6 3.3 %gather_fusion.1 = bf16[512,2048]{1,0:T(8,128)(2,1)} fusion(bf16[128,2048]{1,0:T(8,128)(2,1)S(1)} %bitcast.115, s32[1024]{0:T(1024)S(1)} %pad_clamp_fusion), kind=kCustom, calls=%fused_computation.1 | custom fusion | bytes 4196352 | tf_op jit(solution)/shard_map/gather | solution.py:187
  89.9 4.8 %reshape.146 = f32[128,4,2048]{2,1,0:T(4,128)} reshape(bf16[512,2048]{1,0:T(8,128)(2,1)} %gather_fusion.1) | data formatting | bytes 6291456 | tf_op jit(solution)/shard_map/convert_element_type | solution.py:187
  94.7 6.3 %multiply_reduce_fusion = bf16[128,2048]{1,0:T(8,128)(2,1)} fusion(f32[128,4,2048]{2,1,0:T(4,128)} %reshape.146, f32[128,4]{1,0:T(8,128)S(1)} %copy.87), kind=kLoop, calls=%fused_computation.2 | loop fusion | flops 1835008 | bytes 4720640 | tf_op jit(solution)/shard_map/reduce_sum | solution.py:188
  100.9 4.1 %all-to-all-start.3 = ((bf16[8,16,2048]{2,1,0:T(8,128)(2,1)}), bf16[8,16,2048]{2,1,0:T(8,128)(2,1)}, u32[]{:S(2)}, u32[]{:S(2)}) async-start(bf16[8,16,2048]{2,1,0:T(8,128)(2,1)} %bitcast.126), calls=%async_computation.3 | async-start | bytes 1048576 | tf_op jit(solution)/shard_map/all_to_all | solution.py:47
  105.1 2.4 %fusion.79 = f32[256,256]{1,0:T(8,128)} fusion(bf16[256,2048]{1,0:T(8,128)(2,1)S(1)} %bitcast.118, bf16[2048,256]{1,0:T(8,128)(2,1)} %param.39), kind=kOutput, calls=%fused_computation.129 | convolution fusion | flops 268435456 | bytes 2359296 | tf_op jit(solution)/shard_map/dot_general | solution.py:173
  107.5 3.9 %convolution_convert_fusion = bf16[256,2048]{1,0:T(8,128)(2,1)} fusion(bf16[256,2048]{1,0:T(8,128)(2,1)} %param.41, bf16[256,2048]{1,0:T(8,128)(2,1)S(1)} %bitcast.119, bf16[2048,256]{1,0:T(8,128)(2,1)} %param.40, f32[256,256]{1,0:T(8,128)} %fusion.79), kind=kOutput, calls=%fused_computation.3 | convolution fusion | flops 537788416 | bytes 4456448 | tf_op jit(solution)/shard_map/dot_general | solution.py:176
  111.4 4.0 %all-to-all-done.3 = bf16[8,16,2048]{2,1,0:T(8,128)(2,1)} async-done(((bf16[8,16,2048]{2,1,0:T(8,128)(2,1)}), bf16[8,16,2048]{2,1,0:T(8,128)(2,1)}, u32[]{:S(2)}, u32[]{:S(2)}) %all-to-all-start.3) | async-done | bytes 524320 | tf_op jit(solution)/shard_map/all_to_all | solution.py:47
  115.4 3.7 %all-to-all-start.4 = ((bf16[16,16,2048]{2,1,0:T(8,128)(2,1)}), bf16[16,16,2048]{2,1,0:T(8,128)(2,1)S(1)}, u32[]{:S(2)}, u32[]{:S(2)}) async-start(bf16[16,16,2048]{2,1,0:T(8,128)(2,1)} %bitcast.129), calls=%async_computation.4 | async-start | bytes 2097152 | tf_op jit(solution)/shard_map/all_to_all | solution.py:177
  119.1 1.8 %copy.97 = f32[1,128,512]{2,1,0:T(8,128)} copy(f32[1,128,512]{1,2,0:T(8,128)} %bitcast.125) | data formatting | bytes 524288 | tf_op jit(solution)/shard_map/stack;reshape | solution.py:90
  120.9 0.8 copy.96
  121.7 1.9 %pad_maximum_fusion.1 = f32[2,128,512]{2,1,0:T(8,128)} fusion(f32[1,128,512]{2,1,0:T(8,128)} %copy.97, f32[1,128,512]{2,1,0:T(8,128)} %copy.96), kind=kLoop, calls=%fused_computation.38 | loop fusion | flops 131072 | bytes 1048576 | tf_op jit(solution)/shard_map/stack | solution.py:90
  123.7 1.1 convert_reduce_fusion.2
  124.9 11.8 %all-to-all-done.4 = bf16[16,16,2048]{2,1,0:T(8,128)(2,1)S(1)} async-done(((bf16[16,16,2048]{2,1,0:T(8,128)(2,1)}), bf16[16,16,2048]{2,1,0:T(8,128)(2,1)S(1)}, u32[]{:S(2)}, u32[]{:S(2)}) %all-to-all-start.4) | async-done | bytes 1048608 | tf_op jit(solution)/shard_map/all_to_all | solution.py:177
  136.8 1.6 %add_convert_fusion = bf16[16,2048]{1,0:T(8,128)(2,1)} fusion(f32[16,2048]{1,0:T(8,128)S(1)} %convert_reduce_fusion, f32[16,2048]{1,0:T(8,128)S(1)} %convert_reduce_fusion.2, f32[128,2048]{1,0:T(8,128)} %copy-done.2, s32[]{:T(128)S(6)} %select_n.41, f32[16]{0:T(128)S(1)} %fusion.18), kind=kLoop, calls=%fused_computation.62 | loop fusion | flops 131072 | bytes 458820 | tf_op jit(solution)/shard_map/convert_element_type | solution.py:191
  (81 shorter events, 6.2 us)
Async XLA Ops:
  0.6 68.1 %copy-start = (bf16[1,512,2048]{2,1,0:T(8,128)(2,1)S(1)}, bf16[1,512,2048]{2,1,0:T(8,128)(2,1)}, u32[]{:S(2)}) copy-start(bf16[1,512,2048]{2,1,0:T(8,128)(2,1)} %param.38) | copy-start | bytes 6291460
  0.6 10.7 %copy-start.10 = (s32[128,4]{0,1:T(4,128)S(1)}, s32[128,4]{0,1:T(4,128)}, u32[]{:S(2)}) copy-start(s32[128,4]{0,1:T(4,128)} %param.34) | copy-start | bytes 6148
  2.5 14.9 %all-to-all-start = ((bf16[8,128,256]{2,1,0:T(8,128)(2,1)}), bf16[8,128,256]{2,1,0:T(8,128)(2,1)S(1)}, u32[]{:S(2)}, u32[]{:S(2)}) async-start(bf16[8,128,256]{2,1,0:T(8,128)(2,1)} %broadcast_in_dim.22), calls=%async_computation | async-start | bytes 1048576 | tf_op jit(solution)/shard_map/all_to_all | solution.py:18
  10.5 2.6 %copy-start.13 = (f32[8,64]{1,0:T(8,128)S(1)}, f32[8,64]{1,0:T(8,128)}, u32[]{:S(2)}) copy-start(f32[8,64]{1,0:T(8,128)} %param.26) | copy-start | bytes 6148
  10.5 2.6 %copy-start.14 = (f32[8,64]{1,0:T(8,128)S(1)}, f32[8,64]{1,0:T(8,128)}, u32[]{:S(2)}) copy-start(f32[8,64]{1,0:T(8,128)} %param.25) | copy-start | bytes 6148
  13.3 4.6 %copy-start.11 = (f32[2048]{0:T(1024)S(1)}, f32[2048]{0:T(1024)}, u32[]{:S(2)}) copy-start(f32[2048]{0:T(1024)} %param.22) | copy-start | bytes 24580
  17.4 1.0 copy-start.7
  17.5 1.4 copy-start.8
  17.6 1.9 %copy-start.9 = (f32[2,8,16,64]{3,2,1,0:T(8,128)S(1)}, f32[2,8,16,64]{3,2,1,0:T(8,128)}, u32[]{:S(2)}) copy-start(f32[2,8,16,64]{3,2,1,0:T(8,128)} %param.29) | copy-start | bytes 196612
  18.4 1.4 copy-start.16
  18.4 14.3 %copy-start.3 = (bf16[1024,2048]{1,0:T(8,128)(2,1)S(1)}, bf16[1024,2048]{1,0:T(8,128)(2,1)}, u32[]{:S(2)}) copy-start(bf16[1024,2048]{1,0:T(8,128)(2,1)} %param.31) | copy-start | bytes 12582916
  19.2 14.4 %copy-start.5 = (f32[128,8,64]{0,2,1:T(8,128)}, f32[128,8,64]{0,2,1:T(8,128)S(1)}, u32[]{:S(2)}) copy-start(f32[128,8,64]{0,2,1:T(8,128)S(1)} %fusion.9) | copy-start | bytes 786436
  32.7 1.9 %copy-start.12 = (f32[2048]{0:T(1024)S(1)}, f32[2048]{0:T(1024)}, u32[]{:S(2)}) copy-start(f32[2048]{0:T(1024)} %param.32) | copy-start | bytes 24580
  33.6 1.0 copy-start.2
  36.0 32.3 %copy-start.6 = (bf16[1,2048,512]{2,1,0:T(8,128)(2,1)S(1)}, bf16[1,2048,512]{2,1,0:T(8,128)(2,1)}, u32[]{:S(2)}) copy-start(bf16[1,2048,512]{2,1,0:T(8,128)(2,1)} %param.36) | copy-start | bytes 6291460
  67.1 1.2 copy-start.1
  72.2 14.4 %all-to-all-start.2 = ((bf16[16,8,2048]{2,1,0:T(8,128)(2,1)}), bf16[16,8,2048]{2,1,0:T(8,128)(2,1)S(1)}, u32[]{:S(2)}, u32[]{:S(2)}) async-start(bf16[16,8,2048]{2,1,0:T(8,128)(2,1)} %fusion), calls=%async_computation.2 | async-start | bytes 1048576 | tf_op jit(solution)/shard_map/all_to_all | solution.py:171
  94.7 10.4 %copy-start.4 = (bf16[16,16,2048]{2,1,0:T(8,128)(2,1)S(1)}, bf16[16,16,2048]{2,1,0:T(8,128)(2,1)}, u32[]{:S(2)}) copy-start(bf16[16,16,2048]{2,1,0:T(8,128)(2,1)} %slice.48) | copy-start | bytes 3145732
  100.9 14.5 %all-to-all-start.3 = ((bf16[8,16,2048]{2,1,0:T(8,128)(2,1)}), bf16[8,16,2048]{2,1,0:T(8,128)(2,1)}, u32[]{:S(2)}, u32[]{:S(2)}) async-start(bf16[8,16,2048]{2,1,0:T(8,128)(2,1)} %bitcast.126), calls=%async_computation.3 | async-start | bytes 1048576 | tf_op jit(solution)/shard_map/all_to_all | solution.py:47
  111.4 7.7 %copy-start.15 = (bf16[2048]{0:T(1024)(128)(2,1)S(1)}, bf16[2048]{0:T(1024)(128)(2,1)}, u32[]{:S(2)}) copy-start(bf16[2048]{0:T(1024)(128)(2,1)} %param.33) | copy-start | bytes 12292
  115.4 21.3 %all-to-all-start.4 = ((bf16[16,16,2048]{2,1,0:T(8,128)(2,1)}), bf16[16,16,2048]{2,1,0:T(8,128)(2,1)S(1)}, u32[]{:S(2)}, u32[]{:S(2)}) async-start(bf16[16,16,2048]{2,1,0:T(8,128)(2,1)} %bitcast.129), calls=%async_computation.4 | async-start | bytes 2097152 | tf_op jit(solution)/shard_map/all_to_all | solution.py:177
where the time goes:
time: 139 us; the launch traced here: 138 us
  blocking collectives  43.9 us (32%)
  waiting for transfers between devices  28.1 us (20%)
  local copies, waits for them, and re-layouts  23 us (17%)
  starting transfers between devices  16 us (12%)
  other arithmetic  14.1 us (10%)
  matrix products  12.4 us (9%)
    all_to_all x1, blocking collectives, in_one_piece(): lax.all_to_all(both, axis, split_axis=split_dim, concat_axis=concat_dim,...  31.1 us
    all_gather x1, blocking collectives, per_device(): mixed_rows = lax.all_gather(mixed_part, 'tp', axis=1, tiled=True)  12.8 us
    all_to_all x1, waiting for transfers between devices, per_device(): lax.all_to_all(partial_rows.reshape(ep_count, per_dev, width).astype(jnp....  11.8 us
    all_to_all x1, waiting for transfers between devices, per_device(): lax.all_to_all(computed, 'ep', split_axis=0, concat_axis=0, tiled=True)  8.19 us
    reduce_sum x1, other arithmetic, per_device(): jnp.sum(jnp.where(is_mine, weights, 0.0)[..., None] * picked, axis=1)  6.28 us
    convert_element_type x1, local copies, waits for them, and re-layouts, per_device(): picked = flat_back[jnp.where(is_mine, slot_place, 0)].astype(jnp.float32)  4.75 us
    all_to_all x1, starting transfers between devices, from_everyone(): lax.all_to_all(jnp.broadcast_to(array[None], (length, *array.shape)), axi...  4.58 us
    all_to_all x1, starting transfers between devices, sent_and_summed(): lax.all_to_all(in_blocks(array, dim, length), axis, 0, 0, tiled=True)  4.14 us
  transfers between devices with their start and end apart: 4, of which 4 were waited for; matrix products, arithmetic and copies ran while one was open for 15% of the time, Pallas kernels for 0%

commit v1 on v0

v1 whole, which is shorter than its diff:
```python
import jax
import jax.numpy as jnp
from jax import lax
from jax.experimental import pallas as pl
from jax.experimental.pallas import tpu as pltpu
from jax.sharding import PartitionSpec as P

MESH = pl.DeviceIdType.MESH
norm_eps = 1e-05
routed_scale = 2.5
f32, bf16 = jnp.float32, jnp.bfloat16

TP, EP = 8, 16
ROWS, WIDTH, FEAT = 128, 2048, 256
CH, GROUPS, STATE, GCH = 128, 8, 64, 16
GS = GROUPS * STATE
CAP, OWN = 8, 16
SLOTS = EP * CAP
FF, SF = 512, 256
MIX = CH * TP


def dot(a, b):
    return jnp.dot(a, b, preferred_element_type=f32)


def dot_nt(a, b):
    return lax.dot_general(a, b, (((1,), (1,)), ((), ())), preferred_element_type=f32)


def dot_tn(a, b):
    return lax.dot_general(a, b, (((0,), (0,)), ((), ())), preferred_element_type=f32)


def halves(a):
    high = a.astype(bf16)
    return high, (a - high.astype(f32)).astype(bf16)


def lanes_of_groups(a):
    return jnp.concatenate([a[g : g + 1, :] for g in range(GROUPS)], axis=1)


def block_diagonal(a):
    wide = jnp.concatenate([a] * GROUPS, axis=1)
    row = lax.broadcasted_iota(jnp.int32, (CH, GS), 0) // GCH
    col = lax.broadcasted_iota(jnp.int32, (CH, GS), 1) // STATE
    return jnp.where(row == col, wide, 0.0)


def per_group_rows(a):
    return jnp.broadcast_to(a[:, None, :], (GROUPS, GCH, STATE)).reshape(CH, STATE)


def kernel(
    resid_ref, in_gain_ref, in_w_hbm, state_hbm, decay_ref, freq_ref, step_ref, in_coef_ref,
    out_coef_ref, skip_ref, out_w_hbm, mid_gain_ref, gate_vec_ref, routes_ref, weights_ref,
    eg_hbm, eu_hbm, ed_hbm, sg_hbm, su_hbm, sd_hbm,
    out_ref, new_state_hbm,
    full, in_w, state, new_state, out_w, eg, eu, ed, sg, su, sd,
    mixed, after, mid, outgoing, slots_in, rows_in, hidden, result, returned,
    shidden, partial, partial_in, routed_part, routed_in,
    local_sem, out_sem, s1, r1, s2, r2, s3, r3, s4, r4, s5, r5, s6, r6, s7, r7,
):
    e = lax.axis_index("ep")
    t = lax.axis_index("tp")
    tp_peers = [(d, (e, lax.rem(t + d, TP))) for d in range(1, TP)]
    ep_peers = [(d, (lax.rem(e + d, EP), t)) for d in range(1, EP)]

    barrier = pltpu.get_barrier_semaphore()
    for _, dev in tp_peers + ep_peers:
        pl.semaphore_signal(barrier, inc=1, device_id=dev, device_id_type=MESH)

    fetches = {}
    for i, (name, src, dst) in enumerate([
        ("in_w", in_w_hbm, in_w), ("state", state_hbm, state), ("out_w", out_w_hbm, out_w),
        ("eg", eg_hbm, eg), ("eu", eu_hbm, eu), ("ed", ed_hbm, ed),
        ("sg", sg_hbm, sg), ("su", su_hbm, su), ("sd", sd_hbm, sd),
    ]):
        fetches[name] = pltpu.make_async_copy(src, dst, local_sem.at[i])
        fetches[name].start()

    def send(src, dst, ss, rs, d, dev):
        return pltpu.make_async_remote_copy(
            src_ref=src, dst_ref=dst, send_sem=ss.at[d - 1], recv_sem=rs.at[d - 1],
            device_id=dev, device_id_type=MESH,
        )

    row8 = lax.broadcasted_iota(jnp.int32, (GROUPS, STATE), 0)
    log_step = jnp.zeros((GROUPS, STATE), f32)
    for g in range(GROUPS):
        log_step = jnp.where(row8 == g, step_ref[g], log_step)
    dt = jnp.exp(log_step)
    rate = -decay_ref[...]
    freq = freq_ref[...]
    magnitude = jnp.exp(rate * dt)
    keep_re = magnitude * jnp.cos(freq * dt)
    keep_im = magnitude * jnp.sin(freq * dt)
    denominator = rate * rate + freq * freq
    factor_re = ((keep_re - 1.0) * rate + keep_im * freq) / denominator
    factor_im = (keep_im * rate - (keep_re - 1.0) * freq) / denominator
    fr, fi = per_group_rows(factor_re), per_group_rows(factor_im)
    push_re = block_diagonal(fr * in_coef_ref[0] - fi * in_coef_ref[1])
    push_im = block_diagonal(fr * in_coef_ref[1] + fi * in_coef_ref[0])
    pr_hi, pr_lo = halves(push_re)
    pi_hi, pi_lo = halves(push_im)
    out_re = block_diagonal(out_coef_ref[0]).astype(bf16)
    out_im = block_diagonal(out_coef_ref[1]).astype(bf16)
    kr, ki = lanes_of_groups(keep_re), lanes_of_groups(keep_im)

    slot_row = lax.broadcasted_iota(jnp.int32, (SLOTS, ROWS), 0)
    expert = (slot_row // CAP) * TP + t
    weight_sum = jnp.sum(weights_ref[...], axis=0, keepdims=True)
    weights = weights_ref[...] / weight_sum * routed_scale
    chosen = jnp.zeros((SLOTS, ROWS), f32)
    chosen_weight = jnp.zeros((SLOTS, ROWS), f32)
    for k in range(4):
        same = routes_ref[k : k + 1, :] == expert
        chosen = jnp.where(same, 1.0, chosen)
        chosen_weight = jnp.where(same, weights[k : k + 1, :], chosen_weight)
    earlier = (
        lax.broadcasted_iota(jnp.int32, (ROWS, ROWS), 0)
        < lax.broadcasted_iota(jnp.int32, (ROWS, ROWS), 1)
    )
    before = dot(chosen.astype(bf16), jnp.where(earlier, 1.0, 0.0).astype(bf16))
    rank = (slot_row % CAP).astype(f32)
    holds = (chosen > 0.5) & (before == rank)
    pick = jnp.where(holds, 1.0, 0.0).astype(bf16)
    combine = jnp.where(holds, chosen_weight, 0.0).T
    comb_hi, comb_lo = halves(combine)

    pl.semaphore_wait(barrier, TP - 1 + EP - 1)

    cols = pl.ds(pl.multiple_of(t * FEAT, FEAT), FEAT)
    phase1 = [send(resid_ref, full.at[:, cols], s1, r1, d, dev) for d, dev in tp_peers]
    for c in phase1:
        c.start()
    full[:, cols] = resid_ref[...]
    fetches["state"].wait()
    old_re, old_im = state[0], state[1]
    new_state[0] = kr * old_re - ki * old_im
    new_state[1] = kr * old_im + ki * old_re
    fetches["in_w"].wait()
    for c in phase1:
        c.wait_recv()
    values = full[...].astype(f32)
    mean = jnp.sum(values, axis=1, keepdims=True) * (1.0 / WIDTH)
    square = jnp.sum(values * values, axis=1, keepdims=True) * (1.0 / WIDTH)
    scale = lax.rsqrt(square - mean * mean + norm_eps)
    normed = ((values - mean) * scale * in_gain_ref[...]).astype(bf16)
    drive = dot(normed, in_w[...]).astype(bf16)
    new_re = new_state[0] + (dot(drive, pr_hi) + dot(drive, pr_lo))
    new_im = new_state[1] + (dot(drive, pi_hi) + dot(drive, pi_lo))
    new_state[0] = new_re
    new_state[1] = new_im
    read = dot_nt(new_re.astype(bf16), out_re) - dot_nt(new_im.astype(bf16), out_im)
    read = read + skip_ref[...] * drive.astype(f32)
    mixed_cols = pl.ds(pl.multiple_of(t * CH, CH), CH)
    mixed[:, mixed_cols] = jax.nn.gelu(read, approximate=True).astype(bf16)

    phase2 = [send(mixed.at[:, mixed_cols], mixed.at[:, mixed_cols], s2, r2, d, dev) for d, dev in tp_peers]
    for c in phase2:
        c.start()
    state_out = pltpu.make_async_copy(new_state, new_state_hbm, out_sem)
    state_out.start()
    fetches["out_w"].wait()
    for c in phase2:
        c.wait_recv()

    def mix_columns(j, carry):
        at = pl.ds(pl.multiple_of(j * 256, 256), 256)
        part = full[:, at].astype(f32) + dot(mixed[...], out_w[:, at])
        after[:, at] = part
        return (
            carry[0] + part[:, :128] + part[:, 128:],
            carry[1] + part[:, :128] * part[:, :128] + part[:, 128:] * part[:, 128:],
        )

    zero = jnp.zeros((ROWS, 128), f32)
    total, squares = lax.fori_loop(0, WIDTH // 256, mix_columns, (zero, zero))
    mean = jnp.sum(total, axis=1, keepdims=True) * (1.0 / WIDTH)
    square = jnp.sum(squares, axis=1, keepdims=True) * (1.0 / WIDTH)
    scale = lax.rsqrt(square - mean * mean + norm_eps)

    def norm_columns(j, carry):
        at = pl.ds(pl.multiple_of(j * 256, 256), 256)
        part = ((after[:, at] - mean) * scale * mid_gain_ref[:, at]).astype(bf16)
        mid[:, :, at] = part.reshape(TP, OWN, 256)
        outgoing[:, :, at] = dot(pick, part).astype(bf16).reshape(EP, CAP, 256)
        return carry

    lax.fori_loop(0, WIDTH // 256, norm_columns, 0)

    phase3 = [send(outgoing.at[dev[0]], slots_in.at[e], s3, r3, d, dev) for d, dev in ep_peers]
    phase4 = [send(mid.at[t], rows_in.at[e], s4, r4, d, dev) for d, dev in ep_peers]
    for c in phase3:
        c.start()
    for c in phase4:
        c.start()
    slots_in[e] = outgoing[e]
    own_mid = mid[t]
    rows_in[e] = own_mid
    gate_value = jax.nn.sigmoid(
        jnp.sum(own_mid.astype(f32) * gate_vec_ref[...].astype(f32), axis=1, keepdims=True)
    )

    for name in ("eg", "eu", "ed"):
        fetches[name].wait()
    for c in phase3:
        c.wait_recv()
    rows = slots_in[...].reshape(SLOTS, WIDTH)
    for j in range(FF // 256):
        at = pl.ds(j * 256, 256)
        gate_part = dot(rows, eg[:, at])
        up_part = dot(rows, eu[:, at])
        hidden[:, at] = (jax.nn.silu(gate_part) * up_part).astype(bf16)

    def down_columns(j, carry):
        at = pl.ds(pl.multiple_of(j * 256, 256), 256)
        result[:, :, at] = dot(hidden[...], ed[:, at]).astype(bf16).reshape(EP, CAP, 256)
        return carry

    lax.fori_loop(0, WIDTH // 256, down_columns, 0)
    phase5 = [send(result.at[dev[0]], returned.at[e], s5, r5, d, dev) for d, dev in ep_peers]
    for c in phase5:
        c.start()
    returned[e] = result[e]

    for name in ("sg", "su", "sd"):
        fetches[name].wait()
    for c in phase4:
        c.wait_recv()
    piece = rows_in[...].reshape(EP * OWN, WIDTH)
    gate_part = dot(piece, sg[...])
    up_part = dot(piece, su[...])
    shidden[...] = (jax.nn.silu(gate_part) * up_part).astype(bf16)

    def shared_columns(j, carry):
        at = pl.ds(pl.multiple_of(j * 256, 256), 256)
        partial[:, :, at] = dot(shidden[...], sd[:, at]).astype(bf16).reshape(EP, OWN, 256)
        return carry

    lax.fori_loop(0, WIDTH // 256, shared_columns, 0)
    phase6 = [send(partial.at[dev[0]], partial_in.at[e], s6, r6, d, dev) for d, dev in ep_peers]
    for c in phase6:
        c.start()
    partial_in[e] = partial[e]

    for c in phase5:
        c.wait_recv()

    def combine_columns(j, carry):
        at = pl.ds(pl.multiple_of(j * 256, 256), 256)
        back = returned[:, :, at].reshape(SLOTS, 256)
        part = dot(comb_hi, back) + dot(comb_lo, back)
        routed_part[:, :, at] = part.astype(bf16).reshape(TP, OWN, 256)
        return carry

    lax.fori_loop(0, WIDTH // 256, combine_columns, 0)
    phase7 = [send(routed_part.at[dev[1]], routed_in.at[t], s7, r7, d, dev) for d, dev in tp_peers]
    for c in phase7:
        c.start()
    routed_in[t] = routed_part[t]
    for c in phase7:
        c.wait_recv()
    for c in phase6:
        c.wait_recv()

    own_rows = pl.ds(pl.multiple_of(t * OWN, OWN), OWN)
    routed = jnp.sum(routed_in[...].astype(f32), axis=0)
    shared = jnp.sum(partial_in[...].astype(f32), axis=0)
    out_ref[...] = (after[own_rows, :] + routed + gate_value * shared).astype(bf16)

    for c in phase1 + phase2 + phase3 + phase4 + phase5 + phase6 + phase7:
        c.wait_send()
    state_out.wait()


def per_device(
    residual, in_gain, in_weight, state, decay_rate, frequency, log_step, in_coef, out_coef,
    skip_gain, out_weight, mid_gain, gate_vector, routes, route_weight, expert_gate, expert_up,
    expert_down, shared_gate, shared_up, shared_down,
):
    vmem = pl.BlockSpec(memory_space=pltpu.VMEM)
    smem = pl.BlockSpec(memory_space=pltpu.SMEM)
    hbm = pl.BlockSpec(memory_space=pl.ANY)
    dma = pltpu.SemaphoreType.DMA
    in_coef_rows = jnp.swapaxes(in_coef, 2, 3).reshape(2, CH, STATE)
    out_coef_rows = out_coef.reshape(2, CH, STATE)
    return pl.pallas_call(
        kernel,
        name="layer_step",
        out_shape=(
            jax.ShapeDtypeStruct((OWN, WIDTH), bf16),
            jax.ShapeDtypeStruct((2, ROWS, GS), f32),
        ),
        in_specs=[
            vmem, vmem, hbm, hbm, vmem, vmem, smem, vmem, vmem, vmem, hbm, vmem, vmem, vmem, vmem,
            hbm, hbm, hbm, hbm, hbm, hbm,
        ],
        out_specs=(vmem, hbm),
        scratch_shapes=[
            pltpu.VMEM((ROWS, WIDTH), bf16),
            pltpu.VMEM((WIDTH, CH), bf16),
            pltpu.VMEM((2, ROWS, GS), f32),
            pltpu.VMEM((2, ROWS, GS), f32),
            pltpu.VMEM((MIX, WIDTH), bf16),
            pltpu.VMEM((WIDTH, FF), bf16),
            pltpu.VMEM((WIDTH, FF), bf16),
            pltpu.VMEM((FF, WIDTH), bf16),
            pltpu.VMEM((WIDTH, SF), bf16),
            pltpu.VMEM((WIDTH, SF), bf16),
            pltpu.VMEM((SF, WIDTH), bf16),
            pltpu.VMEM((ROWS, MIX), bf16),
            pltpu.VMEM((ROWS, WIDTH), f32),
            pltpu.VMEM((TP, OWN, WIDTH), bf16),
            pltpu.VMEM((EP, CAP, WIDTH), bf16),
            pltpu.VMEM((EP, CAP, WIDTH), bf16),
            pltpu.VMEM((EP, OWN, WIDTH), bf16),
            pltpu.VMEM((SLOTS, FF), bf16),
            pltpu.VMEM((EP, CAP, WIDTH), bf16),
            pltpu.VMEM((EP, CAP, WIDTH), bf16),
            pltpu.VMEM((EP * OWN, SF), bf16),
            pltpu.VMEM((EP, OWN, WIDTH), bf16),
            pltpu.VMEM((EP, OWN, WIDTH), bf16),
            pltpu.VMEM((TP, OWN, WIDTH), bf16),
            pltpu.VMEM((TP, OWN, WIDTH), bf16),
            dma((9,)), dma,
            dma((TP - 1,)), dma((TP - 1,)),
            dma((TP - 1,)), dma((TP - 1,)),
            dma((EP - 1,)), dma((EP - 1,)),
            dma((EP - 1,)), dma((EP - 1,)),
            dma((EP - 1,)), dma((EP - 1,)),
            dma((EP - 1,)), dma((EP - 1,)),
            dma((TP - 1,)), dma((TP - 1,)),
        ],
        compiler_params=pltpu.CompilerParams(
            collective_id=0, has_side_effects=True, vmem_limit_bytes=60 * 1024 * 1024
        ),
    )(
        residual, in_gain.reshape(1, WIDTH), in_weight, state, decay_rate, frequency, log_step,
        in_coef_rows, out_coef_rows, skip_gain.reshape(1, CH), out_weight,
        mid_gain.reshape(1, WIDTH), gate_vector.reshape(1, WIDTH), routes.T, route_weight.T,
        expert_gate[0], expert_up[0], expert_down[0], shared_gate, shared_up, shared_down,
    )


def solution(mesh):
    return jax.shard_map(
        per_device,
        mesh=mesh,
        in_specs=(
            P("ep", "tp"), P(), P(None, "tp"), P(None, "ep", "tp"), P("tp", None), P("tp", None),
            P("tp"), P(None, "tp", None, None), P(None, "tp", None, None), P("tp"), P(), P(), P(),
            P("ep", None), P("ep", None), P(("ep", "tp"), None, None), P(("ep", "tp"), None, None),
            P(("ep", "tp"), None, None), P(None, "ep"), P(None, "ep"), P("ep", None),
        ),
        out_specs=(P(("ep", "tp"), None), P(None, "ep", "tp")),
        check_vma=False,
    )
```

time: 139 us -> 72.9 us (0.52)
  Pallas kernels: 0 us -> 67.2 us
  blocking collectives: 43.9 us -> 0 us
  waiting for transfers between devices: 28.1 us -> 0 us
  local copies, waits for them, and re-layouts: 23 us -> 4.63 us
  starting transfers between devices: 16 us -> 0 us
  other arithmetic: 14.1 us -> 0 us
  matrix products: 12.4 us -> 0 us
    pallas_call x0 -> x1, Pallas kernels: none -> 67.2 us  [per_device(): pl.pallas_call(kernel, name='layer_step', out_shape=(jax.ShapeDtypeStruct...]
    all_to_all x1 -> x0, blocking collectives: 31.1 us -> none  [in_one_piece(): lax.all_to_all(both, axis, split_axis=split_dim, concat_axis=concat_dim,...]
    all_to_all x4 -> x0, waiting for transfers between devices: 28.1 us -> none  [the longest x1 11.8 us: per_device(): lax.all_to_all(partial_rows.reshape(ep_count, per_dev, width).astype(jnp....]
    all_to_all x4 -> x0, starting transfers between devices: 16 us -> none  [the longest x1 4.58 us: from_everyone(): lax.all_to_all(jnp.broadcast_to(array[None], (length, *array.shape)), axi...]
    all_gather x1 -> x0, blocking collectives: 12.8 us -> none  [per_device(): mixed_rows = lax.all_gather(mixed_part, 'tp', axis=1, tiled=True)]
    dot_general x11 -> x0, matrix products: 12.4 us -> none  [the longest x1 3.91 us: per_device(): jnp.dot(shared_hidden, shared_down, preferred_element_type=jnp.float32)]
    reduce_sum x7 -> x0, other arithmetic: 8.86 us -> none  [the longest x1 6.28 us: per_device(): jnp.sum(jnp.where(is_mine, weights, 0.0)[..., None] * picked, axis=1)]
    convert_element_type x2 -> x0, local copies, waits for them, and re-layouts: 4.84 us -> none  [the longest x1 4.75 us: per_device(): picked = flat_back[jnp.where(is_mine, slot_place, 0)].astype(jnp.float32)]
  transfers between devices with their start and end apart: 4 -> 0, of which waited for: 4 -> 0; matrix products, arithmetic and copies ran while one was open for 15% -> 0% of each run, Pallas kernels for 0% -> 0%
where the time goes in v1:
time: 72.9 us; the launch traced here: 72.4 us
  Pallas kernels  67.2 us (92%)
  local copies, waits for them, and re-layouts  4.63 us (6%)
    pallas_call x1, Pallas kernels, per_device(): pl.pallas_call(kernel, name='layer_step', out_shape=(jax.ShapeDtypeStruct...  67.2 us
    unnamed x2, local copies, waits for them, and re-layouts  3.34 us

profile of v1, /device:TPU:0, one launch (start us, length us, event | category | flops | bytes accessed | tf_op | source)
XLA Modules:
  0.0 72.4 jit_solution(3247521766660807324)
XLA Ops:
  0.6 1.3 %reshape.27.gate_vec_ref = bf16[1,2048]{1,0:T(2,128)(2,1)} reshape(bf16[2048]{0:T(1024)(128)(2,1)} %param.33) | data formatting | bytes 8192 | tf_op jit(solution)/shard_map/reshape | solution.py:343
  1.9 67.2 %layer_step.1 = (bf16[16,2048]{1,0:T(8,128)(2,1)}, f32[2,128,512]{2,1,0:T(8,128)}) custom-call(bf16[128,256]{1,0:T(8,128)(2,1)} %resid_ref.1, f32[1,2048]{1,0:T(1,128)} %bitcast.17, bf16[2048,128]{1,0:T(8,128)(2,1)} %in_w_hbm.1, f32[2,128,512]{2,1,0:T(8,128)} %state_hbm.1, f32[8,64]{1,0:T(8,128)} %decay_ref.1, f32[8,64]{1,0:T(8,128)} %freq_ref.1, ...), custom_call_target="tpu_custom_call" | custom-call | tf_op jit(solution)/shard_map/layer_step/pallas_call | solution.py:290
  69.1 1.5 %copy.25 = bf16[16,2048]{1,0:T(8,128)(2,1)} copy(bf16[16,2048]{1,0:T(8,128)(2,1)} %get-tuple-element.4) | data formatting | bytes 131072
  70.6 1.9 %copy.26 = f32[2,128,512]{2,1,0:T(8,128)} copy(f32[2,128,512]{2,1,0:T(8,128)} %get-tuple-element.5) | data formatting | bytes 1048576

commit v2 on v1

v2 whole, which is shorter than its diff:
```python
import jax
import jax.numpy as jnp
from jax import lax
from jax.experimental import pallas as pl
from jax.experimental.pallas import tpu as pltpu
from jax.sharding import PartitionSpec as P

MESH = pl.DeviceIdType.MESH
norm_eps = 1e-05
routed_scale = 2.5
f32, bf16 = jnp.float32, jnp.bfloat16

TP, EP = 8, 16
ROWS, WIDTH, FEAT = 128, 2048, 256
CH, GROUPS, STATE, GCH = 128, 8, 64, 16
GS = GROUPS * STATE
CAP, OWN = 8, 16
SIDE = 4
HALF = WIDTH // 2
SLOTS = EP * CAP
FF, SF = 512, 256
MIX = CH * TP
VMEM_MIB = 48


def dot(a, b):
    return jnp.dot(a, b, preferred_element_type=f32)


def dot_nt(a, b):
    return lax.dot_general(a, b, (((1,), (1,)), ((), ())), preferred_element_type=f32)


def dot_tn(a, b):
    return lax.dot_general(a, b, (((0,), (0,)), ((), ())), preferred_element_type=f32)


def halves(a):
    high = a.astype(bf16)
    return high, (a - high.astype(f32)).astype(bf16)


def lanes_of_groups(a):
    return jnp.concatenate([a[g : g + 1, :] for g in range(GROUPS)], axis=1)


def block_diagonal(a):
    wide = jnp.concatenate([a] * GROUPS, axis=1)
    row = lax.broadcasted_iota(jnp.int32, (CH, GS), 0) // GCH
    col = lax.broadcasted_iota(jnp.int32, (CH, GS), 1) // STATE
    return jnp.where(row == col, wide, 0.0)


def per_group_rows(a):
    return jnp.broadcast_to(a[:, None, :], (GROUPS, GCH, STATE)).reshape(CH, STATE)


def kernel(
    resid_hbm, in_gain_hbm, in_w_hbm, state_hbm, decay_hbm, freq_hbm, step_hbm, in_coef_hbm,
    out_coef_hbm, skip_hbm, out_w_hbm, mid_gain_hbm, gate_vec_hbm, routes_hbm, weights_hbm,
    eg_hbm, eu_hbm, ed_hbm, sg_hbm, su_hbm, sd_hbm,
    out_ref, new_state_ref,
    resid_ref, in_gain_ref, decay_ref, freq_ref, step_ref, in_coef_ref, out_coef_ref, skip_ref,
    mid_gain_ref, gate_vec_ref, routes_ref, weights_ref,
    full, in_w, state, out_w, eg, eu, ed, sg, su, sd,
    mixed, after, mid, outgoing, slots_in, rows_in, hidden, result, returned,
    shidden, partial, stage_a, stage_b, sum_a, sum_b, final_a, final_b, routed_part, routed_in,
    local_sem, s1, r1, s2, r2, s3, r3, s4, r4, s4f, r4f, s5, r5, s6, r6, s6f, r6f, s7, r7,
):
    e = lax.axis_index("ep")
    t = lax.axis_index("tp")
    z, x = e // SIDE, e % SIDE
    y, core = t // 2, t % 2
    tp_peers = [
        (dy * 2 + dc, (e, ((y + dy) % SIDE) * 2 + (core + dc) % 2))
        for dy in (1, 3, 2, 0) for dc in (0, 1) if dy + dc
    ]
    ep_peers = [
        (dz * SIDE + dx, (((z + dz) % SIDE) * SIDE + (x + dx) % SIDE, t))
        for dz in range(SIDE) for dx in range(SIDE) if dz + dx
    ]
    x_peers = [(d, (z * SIDE + (x + d) % SIDE, t), (x + d) % SIDE) for d in (1, 3, 2)]
    z_peers = [(d, (((z + d) % SIDE) * SIDE + x, t), (z + d) % SIDE) for d in (1, 3, 2)]

    barrier = pltpu.get_barrier_semaphore()
    for _, dev in tp_peers + ep_peers:
        pl.semaphore_signal(barrier, inc=1, device_id=dev, device_id_type=MESH)

    fetches = {}
    for i, (name, src, dst) in enumerate([
        ("resid", resid_hbm, resid_ref), ("decay", decay_hbm, decay_ref),
        ("freq", freq_hbm, freq_ref), ("step", step_hbm, step_ref),
        ("in_coef", in_coef_hbm, in_coef_ref), ("out_coef", out_coef_hbm, out_coef_ref),
        ("routes", routes_hbm, routes_ref), ("weights", weights_hbm, weights_ref),
        ("skip", skip_hbm, skip_ref), ("in_gain", in_gain_hbm, in_gain_ref),
        ("state", state_hbm, state), ("in_w", in_w_hbm, in_w),
        ("mid_gain", mid_gain_hbm, mid_gain_ref), ("gate_vec", gate_vec_hbm, gate_vec_ref),
        ("out_w", out_w_hbm, out_w),
        ("eg", eg_hbm, eg), ("eu", eu_hbm, eu), ("ed", ed_hbm, ed),
        ("sg", sg_hbm, sg), ("su", su_hbm, su), ("sd", sd_hbm, sd),
    ]):
        fetches[name] = pltpu.make_async_copy(src, dst, local_sem.at[i])
        fetches[name].start()

    def fetched(*names):
        for name in names:
            fetches[name].wait()

    def send(src, dst, ss, rs, d, dev):
        return pltpu.make_async_remote_copy(
            src_ref=src, dst_ref=dst, send_sem=ss.at[d], recv_sem=rs.at[d],
            device_id=dev, device_id_type=MESH,
        )

    fetched("decay", "freq", "step", "in_coef", "out_coef")
    own_lane = (
        lax.broadcasted_iota(jnp.int32, (GROUPS, GROUPS), 0)
        == lax.broadcasted_iota(jnp.int32, (GROUPS, GROUPS), 1)
    )
    log_step = jnp.sum(jnp.where(own_lane, step_ref[...], 0.0), axis=1, keepdims=True)
    dt = jnp.exp(log_step)
    rate = -decay_ref[...]
    freq = freq_ref[...]
    magnitude = jnp.exp(rate * dt)
    keep_re = magnitude * jnp.cos(freq * dt)
    keep_im = magnitude * jnp.sin(freq * dt)
    denominator = rate * rate + freq * freq
    factor_re = ((keep_re - 1.0) * rate + keep_im * freq) / denominator
    factor_im = (keep_im * rate - (keep_re - 1.0) * freq) / denominator
    fr, fi = per_group_rows(factor_re), per_group_rows(factor_im)
    push_re = block_diagonal(fr * in_coef_ref[0] - fi * in_coef_ref[1])
    push_im = block_diagonal(fr * in_coef_ref[1] + fi * in_coef_ref[0])
    pr_hi, pr_lo = halves(push_re)
    pi_hi, pi_lo = halves(push_im)
    out_re = block_diagonal(out_coef_ref[0]).astype(bf16)
    out_im = block_diagonal(out_coef_ref[1]).astype(bf16)
    kr, ki = lanes_of_groups(keep_re), lanes_of_groups(keep_im)

    fetched("routes", "weights")
    slot_row = lax.broadcasted_iota(jnp.int32, (SLOTS, ROWS), 0)
    expert = (slot_row // CAP) * TP + t
    weight_sum = jnp.sum(weights_ref[...], axis=0, keepdims=True)
    weights = weights_ref[...] / weight_sum * routed_scale
    chosen = jnp.zeros((SLOTS, ROWS), f32)
    chosen_weight = jnp.zeros((SLOTS, ROWS), f32)
    for k in range(4):
        same = routes_ref[k : k + 1, :] == expert
        chosen = jnp.where(same, 1.0, chosen)
        chosen_weight = jnp.where(same, weights[k : k + 1, :], chosen_weight)
    earlier = (
        lax.broadcasted_iota(jnp.int32, (ROWS, ROWS), 0)
        < lax.broadcasted_iota(jnp.int32, (ROWS, ROWS), 1)
    )
    before = dot(chosen.astype(bf16), jnp.where(earlier, 1.0, 0.0).astype(bf16))
    rank = (slot_row % CAP).astype(f32)
    holds = (chosen > 0.5) & (before == rank)
    pick = jnp.where(holds, 1.0, 0.0).astype(bf16)
    combine = jnp.where(holds, chosen_weight, 0.0).T
    comb_hi, comb_lo = halves(combine)

    pl.semaphore_wait(barrier, TP - 1 + EP - 1)

    cols = pl.ds(pl.multiple_of(t * FEAT, FEAT), FEAT)
    fetched("resid")
    phase1 = [send(resid_ref, full.at[:, cols], s1, r1, d, dev) for d, dev in tp_peers]
    for c in phase1:
        c.start()
    full[:, cols] = resid_ref[...]
    fetched("state", "in_w", "in_gain", "skip")
    old_re, old_im = state[0], state[1]
    new_state_ref[0] = kr * old_re - ki * old_im
    new_state_ref[1] = kr * old_im + ki * old_re
    for c in phase1:
        c.wait_recv()
    values = full[...].astype(f32)
    mean = jnp.sum(values, axis=1, keepdims=True) * (1.0 / WIDTH)
    square = jnp.sum(values * values, axis=1, keepdims=True) * (1.0 / WIDTH)
    scale = lax.rsqrt(square - mean * mean + norm_eps)
    normed = ((values - mean) * scale * in_gain_ref[...]).astype(bf16)
    drive = dot(normed, in_w[...]).astype(bf16)
    new_re = new_state_ref[0] + (dot(drive, pr_hi) + dot(drive, pr_lo))
    new_im = new_state_ref[1] + (dot(drive, pi_hi) + dot(drive, pi_lo))
    new_state_ref[0] = new_re
    new_state_ref[1] = new_im
    read = dot_nt(new_re.astype(bf16), out_re) - dot_nt(new_im.astype(bf16), out_im)
    read = read + skip_ref[...] * drive.astype(f32)
    mixed_cols = pl.ds(pl.multiple_of(t * CH, CH), CH)
    mixed[:, mixed_cols] = jax.nn.gelu(read, approximate=True).astype(bf16)

    phase2 = [send(mixed.at[:, mixed_cols], mixed.at[:, mixed_cols], s2, r2, d, dev) for d, dev in tp_peers]
    for c in phase2:
        c.start()
    fetched("out_w", "mid_gain")
    arrivals = {d: c for (d, _), c in zip(tp_peers, phase2, strict=True)}
    sums = [jnp.zeros((ROWS, 128), f32), jnp.zeros((ROWS, 128), f32)]
    for dy in (0, 1, 3, 2):
        for dc in (0, 1):
            if dy + dc:
                arrivals[dy * 2 + dc].wait_recv()
        deep = pl.ds(pl.multiple_of(((y + SIDE - dy) % SIDE) * 256, 256), 256)
        block = mixed[:, deep]
        for j in range(WIDTH // 256):
            at = pl.ds(j * 256, 256)
            base = full[:, at].astype(f32) if dy == 0 else after[:, at]
            part = base + dot(block, out_w[deep, at])
            after[:, at] = part
            if dy == 2:
                for piece in (part[:, :128], part[:, 128:]):
                    sums[0] = sums[0] + piece
                    sums[1] = sums[1] + piece * piece
    mean = jnp.sum(sums[0], axis=1, keepdims=True) * (1.0 / WIDTH)
    square = jnp.sum(sums[1], axis=1, keepdims=True) * (1.0 / WIDTH)
    scale = lax.rsqrt(square - mean * mean + norm_eps)
    for j in range(WIDTH // 256):
        at = pl.ds(j * 256, 256)
        part = ((after[:, at] - mean) * scale * mid_gain_ref[:, at]).astype(bf16)
        mid[:, :, at] = part.reshape(TP, OWN, 256)
        outgoing[:, :, at] = dot(pick, part).astype(bf16).reshape(EP, CAP, 256)

    half_a, half_b = pl.ds(0, HALF), pl.ds(HALF, HALF)
    phase4 = []
    for k, (a, b) in enumerate(((half_a, half_b), (half_b, half_a))):
        for (d, dev, _), (_, dev_z, _) in zip(x_peers, z_peers, strict=True):
            phase4 += [
                send(mid.at[t, :, a], rows_in.at[e, :, a], s4, r4, k * 8 + d, dev),
                send(mid.at[t, :, b], rows_in.at[e, :, b], s4, r4, k * 8 + 4 + d, dev_z),
            ]
    phase3 = [send(outgoing.at[dev[0]], slots_in.at[e], s3, r3, d, dev) for d, dev in ep_peers]
    for c in phase4:
        c.start()
    for c in phase3:
        c.start()
    slots_in[e] = outgoing[e]
    own_mid = mid[t]
    rows_in[e] = own_mid
    fetched("gate_vec")
    gate_vec = jnp.concatenate([gate_vec_ref[i : i + 1, :] for i in range(WIDTH // 128)], axis=1)
    gate_value = jax.nn.sigmoid(
        jnp.sum(own_mid.astype(f32) * gate_vec.astype(f32), axis=1, keepdims=True)
    )
    forwards = []
    for i, d in enumerate((1, 3, 2)):
        phase4[2 * i].wait_recv()
        from_x = z * SIDE + (x + SIDE - d) % SIDE
        for dz, dev, _ in z_peers:
            block = rows_in.at[from_x, :, half_a]
            forwards.append(send(block, block, s4f, r4f, d * 4 + dz, dev))
            forwards[-1].start()
        phase4[2 * i + 1].wait_recv()
        from_z = ((z + SIDE - d) % SIDE) * SIDE + x
        for dx, dev, _ in x_peers:
            block = rows_in.at[from_z, :, half_b]
            forwards.append(send(block, block, s4f, r4f, 16 + d * 4 + dx, dev))
            forwards[-1].start()

    fetched("eg", "eu", "ed")
    for c in phase3:
        c.wait_recv()
    rows = slots_in[...].reshape(SLOTS, WIDTH)
    for j in range(FF // 256):
        at = pl.ds(j * 256, 256)
        gate_part = dot(rows, eg[:, at])
        up_part = dot(rows, eu[:, at])
        hidden[:, at] = (jax.nn.silu(gate_part) * up_part).astype(bf16)

    for j in range(WIDTH // 256):
        at = pl.ds(j * 256, 256)
        result[:, :, at] = dot(hidden[...], ed[:, at]).astype(bf16).reshape(EP, CAP, 256)

    phase5 = [send(result.at[dev[0]], returned.at[e], s5, r5, d, dev) for d, dev in ep_peers]
    for c in phase5:
        c.start()
    returned[e] = result[e]

    fetched("sg", "su", "sd")
    for c in phase4[6:] + forwards:
        c.wait_recv()
    piece = rows_in[...].reshape(EP * OWN, WIDTH)
    gate_part = dot(piece, sg[...])
    up_part = dot(piece, su[...])
    shidden[...] = (jax.nn.silu(gate_part) * up_part).astype(bf16)

    grid = (SIDE, SIDE, OWN)
    phase6 = []
    for half in (0, 1):
        for j in range(HALF // 256):
            at = pl.ds(half * HALF + j * 256, 256)
            partial[:, :, :, at] = dot(shidden[...], sd[:, at]).astype(bf16).reshape(*grid, 256)
        if half == 0:
            begun = [
                send(partial.at[there, :, :, half_a], stage_a.at[d - 1], s6, r6, d, dev)
                for d, dev, there in z_peers
            ]
        else:
            begun = [
                send(partial.at[:, there, :, half_b], stage_b.at[d - 1], s6, r6, 4 + d, dev)
                for d, dev, there in x_peers
            ]
        for c in begun:
            c.start()
        phase6 += begun

    for c in phase5:
        c.wait_recv()

    for j in range(WIDTH // 256):
        at = pl.ds(j * 256, 256)
        back = returned[:, :, at].reshape(SLOTS, 256)
        part = dot(comb_hi, back) + dot(comb_lo, back)
        routed_part[:, :, at] = part.astype(bf16).reshape(TP, OWN, 256)

    phase7 = [send(routed_part.at[dev[1]], routed_in.at[t], s7, r7, d, dev) for d, dev in tp_peers]
    for c in phase7:
        c.start()
    routed_in[t] = routed_part[t]
    for c in phase6[:3]:
        c.wait_recv()
    total = partial[z, :, :, half_a].astype(f32)
    for d in range(3):
        total = total + stage_a[d].astype(f32)
    sum_a[...] = total.astype(bf16)
    phase6f = [send(sum_a.at[there], final_a.at[d - 1], s6f, r6f, d, dev) for d, dev, there in x_peers]
    for c in phase6f:
        c.start()
    for c in phase6[3:]:
        c.wait_recv()
    total = partial[:, x, :, half_b].astype(f32)
    for d in range(3):
        total = total + stage_b[d].astype(f32)
    sum_b[...] = total.astype(bf16)
    begun = [send(sum_b.at[there], final_b.at[d - 1], s6f, r6f, 4 + d, dev) for d, dev, there in z_peers]
    for c in begun:
        c.start()
    phase6f += begun
    for c in phase7:
        c.wait_recv()
    own_rows = pl.ds(pl.multiple_of(t * OWN, OWN), OWN)
    routed = jnp.sum(routed_in[...].astype(f32), axis=0) + after[own_rows, :]
    for c in phase6f:
        c.wait_recv()
    for at, own, others in (
        (half_a, sum_a[x], final_a), (half_b, sum_b[z], final_b),
    ):
        shared = own.astype(f32) + jnp.sum(others[...].astype(f32), axis=0)
        begin = at.start
        out_ref[:, at] = (routed[:, begin : begin + HALF] + gate_value * shared).astype(bf16)

    everything = phase1 + phase2 + phase3 + phase4 + forwards + phase5 + phase6 + phase6f + phase7
    for c in everything:
        c.wait_send()


def per_device(
    residual, in_gain, in_weight, state, decay_rate, frequency, log_step, in_coef, out_coef,
    skip_gain, out_weight, mid_gain, gate_vector, routes, route_weight, expert_gate, expert_up,
    expert_down, shared_gate, shared_up, shared_down,
):
    vmem = pl.BlockSpec(memory_space=pltpu.VMEM)
    hbm = pl.BlockSpec(memory_space=pltpu.HBM)
    dma = pltpu.SemaphoreType.DMA
    in_coef_rows = jnp.swapaxes(in_coef, 2, 3).reshape(2, CH, STATE)
    out_coef_rows = out_coef.reshape(2, CH, STATE)
    call = pl.pallas_call(
        kernel,
        name="layer_step",
        out_shape=(
            pltpu.VMEM((OWN, WIDTH), bf16),
            pltpu.VMEM((2, ROWS, GS), f32),
        ),
        in_specs=[hbm] * 21,
        out_specs=(vmem, vmem),
        scratch_shapes=[
            pltpu.VMEM((ROWS, FEAT), bf16),
            pltpu.VMEM((1, WIDTH), f32),
            pltpu.VMEM((GROUPS, STATE), f32),
            pltpu.VMEM((GROUPS, STATE), f32),
            pltpu.VMEM((1, GROUPS), f32),
            pltpu.VMEM((2, CH, STATE), f32),
            pltpu.VMEM((2, CH, STATE), f32),
            pltpu.VMEM((1, CH), f32),
            pltpu.VMEM((1, WIDTH), f32),
            pltpu.VMEM((WIDTH // 128, 128), bf16),
            pltpu.VMEM((4, ROWS), jnp.int32),
            pltpu.VMEM((4, ROWS), f32),
            pltpu.VMEM((ROWS, WIDTH), bf16),
            pltpu.VMEM((WIDTH, CH), bf16),
            pltpu.VMEM((2, ROWS, GS), f32),
            pltpu.VMEM((MIX, WIDTH), bf16),
            pltpu.VMEM((WIDTH, FF), bf16),
            pltpu.VMEM((WIDTH, FF), bf16),
            pltpu.VMEM((FF, WIDTH), bf16),
            pltpu.VMEM((WIDTH, SF), bf16),
            pltpu.VMEM((WIDTH, SF), bf16),
            pltpu.VMEM((SF, WIDTH), bf16),
            pltpu.VMEM((ROWS, MIX), bf16),
            pltpu.VMEM((ROWS, WIDTH), f32),
            pltpu.VMEM((TP, OWN, WIDTH), bf16),
            pltpu.VMEM((EP, CAP, WIDTH), bf16),
            pltpu.VMEM((EP, CAP, WIDTH), bf16),
            pltpu.VMEM((EP, OWN, WIDTH), bf16),
            pltpu.VMEM((SLOTS, FF), bf16),
            pltpu.VMEM((EP, CAP, WIDTH), bf16),
            pltpu.VMEM((EP, CAP, WIDTH), bf16),
            pltpu.VMEM((EP * OWN, SF), bf16),
            pltpu.VMEM((SIDE, SIDE, OWN, WIDTH), bf16),
            pltpu.VMEM((SIDE - 1, SIDE, OWN, HALF), bf16),
            pltpu.VMEM((SIDE - 1, SIDE, OWN, HALF), bf16),
            pltpu.VMEM((SIDE, OWN, HALF), bf16),
            pltpu.VMEM((SIDE, OWN, HALF), bf16),
            pltpu.VMEM((SIDE - 1, OWN, HALF), bf16),
            pltpu.VMEM((SIDE - 1, OWN, HALF), bf16),
            pltpu.VMEM((TP, OWN, WIDTH), bf16),
            pltpu.VMEM((TP, OWN, WIDTH), bf16),
            dma((21,)),
            dma((TP,)), dma((TP,)),
            dma((TP,)), dma((TP,)),
            dma((EP,)), dma((EP,)),
            dma((16,)), dma((16,)),
            dma((32,)), dma((32,)),
            dma((EP,)), dma((EP,)),
            dma((8,)), dma((8,)),
            dma((8,)), dma((8,)),
            dma((TP,)), dma((TP,)),
        ],
        compiler_params=pltpu.CompilerParams(
            collective_id=0, has_side_effects=True, vmem_limit_bytes=VMEM_MIB * 1024 * 1024
        ),
    )
    operands = (
        residual, in_gain.reshape(1, WIDTH), in_weight, state, decay_rate, frequency,
        log_step.reshape(1, GROUPS), in_coef_rows, out_coef_rows, skip_gain.reshape(1, CH),
        out_weight, mid_gain.reshape(1, WIDTH), gate_vector.reshape(WIDTH // 128, 128), routes.T,
        route_weight.T, expert_gate[0], expert_up[0], expert_down[0], shared_gate, shared_up,
        shared_down,
    )
    return call(*[pltpu.with_memory_space_constraint(a, pltpu.HBM) for a in operands])


def solution(mesh):
    return jax.shard_map(
        per_device,
        mesh=mesh,
        in_specs=(
            P("ep", "tp"), P(), P(None, "tp"), P(None, "ep", "tp"), P("tp", None), P("tp", None),
            P("tp"), P(None, "tp", None, None), P(None, "tp", None, None), P("tp"), P(), P(), P(),
            P("ep", None), P("ep", None), P(("ep", "tp"), None, None), P(("ep", "tp"), None, None),
            P(("ep", "tp"), None, None), P(None, "ep"), P(None, "ep"), P("ep", None),
        ),
        out_specs=(P(("ep", "tp"), None), P(None, "ep", "tp")),
        check_vma=False,
    )
```

time: 72.9 us -> 58.6 us (0.80)
  Pallas kernels: 67.2 us -> 56.4 us
  local copies, waits for them, and re-layouts: 4.63 us -> 1.42 us
    pallas_call x1, Pallas kernels: 67.2 us -> 56.4 us  [per_device(): call(*[pltpu.with_memory_space_constraint(a, pltpu.HBM) for a in operands])]
    unnamed x2, local copies, waits for them, and re-layouts: 3.34 us -> 1.42 us
    reshape x1 -> x0, local copies, waits for them, and re-layouts: 1.29 us -> none  [per_device(): gate_vector.reshape(1, WIDTH)]
where the time goes in v2:
time: 58.6 us; the launch traced here: 58.5 us
  Pallas kernels  56.4 us (96%)
  local copies, waits for them, and re-layouts  1.42 us (2%)
  between operations  0.65 us (1%)
    pallas_call x1, Pallas kernels, per_device(): call(*[pltpu.with_memory_space_constraint(a, pltpu.HBM) for a in operands])  56.4 us
    unnamed x2, local copies, waits for them, and re-layouts  1.42 us

profile of v2, /device:TPU:0, one launch (start us, length us, event | category | flops | bytes accessed | tf_op | source)
XLA Modules:
  0.0 58.5 jit_solution(6194439844889444402)
XLA Ops:
  0.6 56.4 %layer_step.1 = (bf16[16,2048]{1,0:T(8,128)(2,1)S(1)}, f32[2,128,512]{2,1,0:T(8,128)S(1)}) custom-call(bf16[128,256]{1,0:T(8,128)(2,1)} %resid_hbm.1, f32[1,2048]{1,0:T(1,128)} %bitcast.19, bf16[2048,128]{1,0:T(8,128)(2,1)} %in_w_hbm.1, f32[2,128,512]{2,1,0:T(8,128)} %state_hbm.1, f32[8,64]{1,0:T(8,128)} %decay_hbm.1, f32[8,64]{1,0:T(8,128)} %freq_hbm.1, ...), custom_call_target="tpu_custom_call" | custom-call | tf_op jit(solution)/shard_map/layer_step/pallas_call | solution.py:436
  57.0 0.6 %copy.25 = bf16[16,2048]{1,0:T(8,128)(2,1)} copy(bf16[16,2048]{1,0:T(8,128)(2,1)S(1)} %get-tuple-element.2) | data formatting | bytes 131072
  57.7 0.8 %copy.26 = f32[2,128,512]{2,1,0:T(8,128)} copy(f32[2,128,512]{2,1,0:T(8,128)S(1)} %get-tuple-element.3) | data formatting | bytes 1048576

commit v3 on v2

--- a/solution.py
+++ b/solution.py
@@ -63,9 +63,10 @@
     resid_ref, in_gain_ref, decay_ref, freq_ref, step_ref, in_coef_ref, out_coef_ref, skip_ref,
     mid_gain_ref, gate_vec_ref, routes_ref, weights_ref,
     full, in_w, state, out_w, eg, eu, ed, sg, su, sd,
-    mixed, after, mid, outgoing, slots_in, rows_in, hidden, result, returned,
-    shidden, partial, stage_a, stage_b, sum_a, sum_b, final_a, final_b, routed_part, routed_in,
-    local_sem, s1, r1, s2, r2, s3, r3, s4, r4, s4f, r4f, s5, r5, s6, r6, s6f, r6f, s7, r7,
+    mixed, after, mid, outgoing, slots_in, resid_in, mixed_in, after_in, piece, hidden, result, returned,
+    shidden, partial, stage_a, stage_b, sum_a, sum_b, final_a, final_b,
+    routed_part, core_in, core_sum, routed_in,
+    local_sem, s1, r1, s2, r2, se, re, sl, rl, s3, r3, s5, r5, s6, r6, s6f, r6f, s7, r7,
 ):
     e = lax.axis_index("ep")
     t = lax.axis_index("tp")
@@ -81,6 +82,8 @@
     ]
     x_peers = [(d, (z * SIDE + (x + d) % SIDE, t), (x + d) % SIDE) for d in (1, 3, 2)]
     z_peers = [(d, (((z + d) % SIDE) * SIDE + x, t), (z + d) % SIDE) for d in (1, 3, 2)]
+    y_peers = [(d, (e, ((y + d) % SIDE) * 2 + core), (y + d) % SIDE) for d in (1, 3, 2)]
+    partner = (e, y * 2 + (1 - core))
 
     barrier = pltpu.get_barrier_semaphore()
     for _, dev in tp_peers + ep_peers:
@@ -107,10 +110,25 @@
             fetches[name].wait()
 
     def send(src, dst, ss, rs, d, dev):
-        return pltpu.make_async_remote_copy(
-            src_ref=src, dst_ref=dst, send_sem=ss.at[d], recv_sem=rs.at[d],
+        copy = pltpu.make_async_remote_copy(
+            src_ref=src, dst_ref=dst, send_sem=ss, recv_sem=rs.at[d],
             device_id=dev, device_id_type=MESH,
         )
+        copy.start()
+
+    def all_of(ref, sem):
+        pltpu.make_async_copy(ref, ref, sem).wait()
+
+    own_rows = pl.ds(pl.multiple_of(t * OWN, OWN), OWN)
+
+    pl.semaphore_wait(barrier, TP - 1 + EP - 1)
+
+    fetched("resid")
+    cols = pl.ds(pl.multiple_of(t * FEAT, FEAT), FEAT)
+    for d, dev, _ in y_peers:
+        send(resid_ref, full.at[:, cols], s1, r1, d, dev)
+    send(resid_ref, full.at[:, cols], s1, r1, 0, partner)
+    full[:, cols] = resid_ref[...]
 
     fetched("decay", "freq", "step", "in_coef", "out_coef")
     own_lane = (
@@ -158,20 +176,36 @@
     combine = jnp.where(holds, chosen_weight, 0.0).T
     comb_hi, comb_lo = halves(combine)
 
-    pl.semaphore_wait(barrier, TP - 1 + EP - 1)
-
-    cols = pl.ds(pl.multiple_of(t * FEAT, FEAT), FEAT)
-    fetched("resid")
-    phase1 = [send(resid_ref, full.at[:, cols], s1, r1, d, dev) for d, dev in tp_peers]
-    for c in phase1:
-        c.start()
-    full[:, cols] = resid_ref[...]
     fetched("state", "in_w", "in_gain", "skip")
     old_re, old_im = state[0], state[1]
     new_state_ref[0] = kr * old_re - ki * old_im
     new_state_ref[1] = kr * old_im + ki * old_re
-    for c in phase1:
-        c.wait_recv()
+    for d in (1, 3, 2):
+        theirs = pl.ds(pl.multiple_of((((y + SIDE - d) % SIDE) * 2 + core) * FEAT, FEAT), FEAT)
+        all_of(full.at[:, theirs], r1.at[d])
+        send(full.at[:, theirs], full.at[:, theirs], s1, r1, 0, partner)
+    all_of(full.at[:, pl.ds(0, SIDE * FEAT)], r1.at[0])
+
+    def first_step(src, dst, width, ss, rs):
+        left, right = pl.ds(0, width), pl.ds(width, width)
+        for k, (a, b) in enumerate(((left, right), (right, left))):
+            for (d, dev_x, _), (_, dev_z, _) in zip(x_peers, z_peers, strict=True):
+                send(src.at[own_rows, a], dst.at[e, :, a], ss, rs, d if k == 0 else 0, dev_x)
+                send(src.at[own_rows, b], dst.at[e, :, b], ss, rs, 4 + d if k == 0 else 0, dev_z)
+
+    def second_step(dst, width, ss, rs):
+        left, right = pl.ds(0, width), pl.ds(width, width)
+        for d in (1, 3, 2):
+            block = dst.at[z * SIDE + (x + SIDE - d) % SIDE, :, left]
+            all_of(block, rs.at[d])
+            for _, dev, _ in z_peers:
+                send(block, block, ss, rs, 0, dev)
+            block = dst.at[((z + SIDE - d) % SIDE) * SIDE + x, :, right]
+            all_of(block, rs.at[4 + d])
+            for _, dev, _ in x_peers:
+                send(block, block, ss, rs, 0, dev)
+
+    first_step(full, resid_in, HALF, se, re)
     values = full[...].astype(f32)
     mean = jnp.sum(values, axis=1, keepdims=True) * (1.0 / WIDTH)
     square = jnp.sum(values * values, axis=1, keepdims=True) * (1.0 / WIDTH)
@@ -187,17 +221,21 @@
     mixed_cols = pl.ds(pl.multiple_of(t * CH, CH), CH)
     mixed[:, mixed_cols] = jax.nn.gelu(read, approximate=True).astype(bf16)
 
-    phase2 = [send(mixed.at[:, mixed_cols], mixed.at[:, mixed_cols], s2, r2, d, dev) for d, dev in tp_peers]
-    for c in phase2:
-        c.start()
+    for d, dev in tp_peers:
+        send(mixed.at[:, mixed_cols], mixed.at[:, mixed_cols], s2, r2, d // 2, dev)
+    resid_in[e] = full[own_rows, :]
     fetched("out_w", "mid_gain")
-    arrivals = {d: c for (d, _), c in zip(tp_peers, phase2, strict=True)}
     sums = [jnp.zeros((ROWS, 128), f32), jnp.zeros((ROWS, 128), f32)]
     for dy in (0, 1, 3, 2):
-        for dc in (0, 1):
-            if dy + dc:
-                arrivals[dy * 2 + dc].wait_recv()
         deep = pl.ds(pl.multiple_of(((y + SIDE - dy) % SIDE) * 256, 256), 256)
+        if dy:
+            all_of(mixed.at[:, deep], r2.at[dy])
+        else:
+            other = pl.ds(pl.multiple_of((y * 2 + (1 - core)) * CH, CH), CH)
+            all_of(mixed.at[:, other], r2.at[0])
+        if dy == 2:
+            first_step(mixed, mixed_in, MIX // 2, sl, rl)
+            mixed_in[e] = mixed[own_rows, :]
         block = mixed[:, deep]
         for j in range(WIDTH // 256):
             at = pl.ds(j * 256, 256)
@@ -205,9 +243,11 @@
             part = base + dot(block, out_w[deep, at])
             after[:, at] = part
             if dy == 2:
-                for piece in (part[:, :128], part[:, 128:]):
-                    sums[0] = sums[0] + piece
-                    sums[1] = sums[1] + piece * piece
+                for lanes in (part[:, :128], part[:, 128:]):
+                    sums[0] = sums[0] + lanes
+                    sums[1] = sums[1] + lanes * lanes
+        if dy == 0:
+            second_step(resid_in, HALF, se, re)
     mean = jnp.sum(sums[0], axis=1, keepdims=True) * (1.0 / WIDTH)
     square = jnp.sum(sums[1], axis=1, keepdims=True) * (1.0 / WIDTH)
     scale = lax.rsqrt(square - mean * mean + norm_eps)
@@ -217,45 +257,19 @@
         mid[:, :, at] = part.reshape(TP, OWN, 256)
         outgoing[:, :, at] = dot(pick, part).astype(bf16).reshape(EP, CAP, 256)
 
-    half_a, half_b = pl.ds(0, HALF), pl.ds(HALF, HALF)
-    phase4 = []
-    for k, (a, b) in enumerate(((half_a, half_b), (half_b, half_a))):
-        for (d, dev, _), (_, dev_z, _) in zip(x_peers, z_peers, strict=True):
-            phase4 += [
-                send(mid.at[t, :, a], rows_in.at[e, :, a], s4, r4, k * 8 + d, dev),
-                send(mid.at[t, :, b], rows_in.at[e, :, b], s4, r4, k * 8 + 4 + d, dev_z),
-            ]
-    phase3 = [send(outgoing.at[dev[0]], slots_in.at[e], s3, r3, d, dev) for d, dev in ep_peers]
-    for c in phase4:
-        c.start()
-    for c in phase3:
-        c.start()
+    for d, dev in ep_peers:
+        send(outgoing.at[dev[0]], slots_in.at[e], s3, r3, 0, dev)
     slots_in[e] = outgoing[e]
     own_mid = mid[t]
-    rows_in[e] = own_mid
     fetched("gate_vec")
     gate_vec = jnp.concatenate([gate_vec_ref[i : i + 1, :] for i in range(WIDTH // 128)], axis=1)
     gate_value = jax.nn.sigmoid(
         jnp.sum(own_mid.astype(f32) * gate_vec.astype(f32), axis=1, keepdims=True)
     )
-    forwards = []
-    for i, d in enumerate((1, 3, 2)):
-        phase4[2 * i].wait_recv()
-        from_x = z * SIDE + (x + SIDE - d) % SIDE
-        for dz, dev, _ in z_peers:
-            block = rows_in.at[from_x, :, half_a]
-            forwards.append(send(block, block, s4f, r4f, d * 4 + dz, dev))
-            forwards[-1].start()
-        phase4[2 * i + 1].wait_recv()
-        from_z = ((z + SIDE - d) % SIDE) * SIDE + x
-        for dx, dev, _ in x_peers:
-            block = rows_in.at[from_z, :, half_b]
-            forwards.append(send(block, block, s4f, r4f, 16 + d * 4 + dx, dev))
-            forwards[-1].start()
+    second_step(mixed_in, MIX // 2, sl, rl)
 
     fetched("eg", "eu", "ed")
-    for c in phase3:
-        c.wait_recv()
+    all_of(slots_in.at[pl.ds(0, EP - 1)], r3.at[0])
     rows = slots_in[...].reshape(SLOTS, WIDTH)
     for j in range(FF // 256):
         at = pl.ds(j * 256, 256)
@@ -267,77 +281,76 @@
         at = pl.ds(j * 256, 256)
         result[:, :, at] = dot(hidden[...], ed[:, at]).astype(bf16).reshape(EP, CAP, 256)
 
-    phase5 = [send(result.at[dev[0]], returned.at[e], s5, r5, d, dev) for d, dev in ep_peers]
-    for c in phase5:
-        c.start()
+    for d, dev in ep_peers:
+        send(result.at[dev[0]], returned.at[e], s5, r5, 0, dev)
     returned[e] = result[e]
 
     fetched("sg", "su", "sd")
-    for c in phase4[6:] + forwards:
-        c.wait_recv()
-    piece = rows_in[...].reshape(EP * OWN, WIDTH)
-    gate_part = dot(piece, sg[...])
-    up_part = dot(piece, su[...])
+    all_of(resid_in.at[pl.ds(0, 12)], re.at[0])
+    all_of(mixed_in.at[pl.ds(0, 12)], rl.at[0])
+    channels = mixed_in[...].reshape(EP * OWN, MIX)
+    sums = [jnp.zeros((EP * OWN, 128), f32), jnp.zeros((EP * OWN, 128), f32)]
+    for j in range(WIDTH // 256):
+        at = pl.ds(j * 256, 256)
+        part = resid_in[:, :, at].reshape(EP * OWN, 256).astype(f32) + dot(channels, out_w[:, at])
+        after_in[:, at] = part
+        for lanes in (part[:, :128], part[:, 128:]):
+            sums[0] = sums[0] + lanes
+            sums[1] = sums[1] + lanes * lanes
+    mean = jnp.sum(sums[0], axis=1, keepdims=True) * (1.0 / WIDTH)
+    square = jnp.sum(sums[1], axis=1, keepdims=True) * (1.0 / WIDTH)
+    scale = lax.rsqrt(square - mean * mean + norm_eps)
+    for j in range(WIDTH // 256):
+        at = pl.ds(j * 256, 256)
+        piece[:, at] = ((after_in[:, at] - mean) * scale * mid_gain_ref[:, at]).astype(bf16)
+    gate_part = dot(piece[...], sg[...])
+    up_part = dot(piece[...], su[...])
     shidden[...] = (jax.nn.silu(gate_part) * up_part).astype(bf16)
 
     grid = (SIDE, SIDE, OWN)
-    phase6 = []
+    half_a, half_b = pl.ds(0, HALF), pl.ds(HALF, HALF)
     for half in (0, 1):
         for j in range(HALF // 256):
             at = pl.ds(half * HALF + j * 256, 256)
             partial[:, :, :, at] = dot(shidden[...], sd[:, at]).astype(bf16).reshape(*grid, 256)
         if half == 0:
-            begun = [
-                send(partial.at[there, :, :, half_a], stage_a.at[d - 1], s6, r6, d, dev)
-                for d, dev, there in z_peers
-            ]
+            for d, dev, there in z_peers:
+                send(partial.at[there, :, :, half_a], stage_a.at[d - 1], s6.at[0], r6, 0, dev)
         else:
-            begun = [
-                send(partial.at[:, there, :, half_b], stage_b.at[d - 1], s6, r6, 4 + d, dev)
-                for d, dev, there in x_peers
-            ]
-        for c in begun:
-            c.start()
-        phase6 += begun
-
-    for c in phase5:
-        c.wait_recv()
+            for d, dev, there in x_peers:
+                send(partial.at[:, there, :, half_b], stage_b.at[d - 1], s6.at[1], r6, 1, dev)
+
+    all_of(returned.at[pl.ds(0, EP - 1)], r5.at[0])
 
     for j in range(WIDTH // 256):
         at = pl.ds(j * 256, 256)
         back = returned[:, :, at].reshape(SLOTS, 256)
         part = dot(comb_hi, back) + dot(comb_lo, back)
-        routed_part[:, :, at] = part.astype(bf16).reshape(TP, OWN, 256)
-
-    phase7 = [send(routed_part.at[dev[1]], routed_in.at[t], s7, r7, d, dev) for d, dev in tp_peers]
-    for c in phase7:
-        c.start()
-    routed_in[t] = routed_part[t]
-    for c in phase6[:3]:
-        c.wait_recv()
+        routed_part[:, :, :, at] = part.astype(bf16).reshape(SIDE, 2, OWN, 256)
+
+    send(routed_part.at[:, 1 - core], core_in, s7.at[0], r7, 0, partner)
+    all_of(core_in, r7.at[0])
+    core_sum[...] = (routed_part[:, core].astype(f32) + core_in[...].astype(f32)).astype(bf16)
+    for d, dev, there in y_peers:
+        send(core_sum.at[there], routed_in.at[d - 1], s7.at[1], r7, 1, dev)
+    all_of(stage_a, r6.at[0])
     total = partial[z, :, :, half_a].astype(f32)
     for d in range(3):
         total = total + stage_a[d].astype(f32)
     sum_a[...] = total.astype(bf16)
-    phase6f = [send(sum_a.at[there], final_a.at[d - 1], s6f, r6f, d, dev) for d, dev, there in x_peers]
-    for c in phase6f:
-        c.start()
-    for c in phase6[3:]:
-        c.wait_recv()
+    for d, dev, there in x_peers:
+        send(sum_a.at[there], final_a.at[d - 1], s6f.at[0], r6f, 0, dev)
+    all_of(stage_b, r6.at[1])
     total = partial[:, x, :, half_b].astype(f32)
     for d in range(3):
         total = total + stage_b[d].astype(f32)
     sum_b[...] = total.astype(bf16)
-    begun = [send(sum_b.at[there], final_b.at[d - 1], s6f, r6f, 4 + d, dev) for d, dev, there in z_peers]
-    for c in begun:
-        c.start()
-    phase6f += begun
-    for c in phase7:
-        c.wait_recv()
-    own_rows = pl.ds(pl.multiple_of(t * OWN, OWN), OWN)
-    routed = jnp.sum(routed_in[...].astype(f32), axis=0) + after[own_rows, :]
-    for c in phase6f:
-        c.wait_recv()
+    for d, dev, there in z_peers:
+        send(sum_b.at[there], final_b.at[d - 1], s6f.at[1], r6f, 1, dev)
+    all_of(routed_in, r7.at[1])
+    routed = core_sum[y].astype(f32) + jnp.sum(routed_in[...].astype(f32), axis=0) + after[own_rows, :]
+    all_of(final_a, r6f.at[0])
+    all_of(final_b, r6f.at[1])
     for at, own, others in (
         (half_a, sum_a[x], final_a), (half_b, sum_b[z], final_b),
     ):
@@ -345,9 +358,18 @@
         begin = at.start
         out_ref[:, at] = (routed[:, begin : begin + HALF] + gate_value * shared).astype(bf16)
 
-    everything = phase1 + phase2 + phase3 + phase4 + forwards + phase5 + phase6 + phase6f + phase7
-    for c in everything:
-        c.wait_send()
+    all_of(full.at[:, pl.ds(0, 7 * FEAT)], s1)
+    all_of(mixed.at[:, pl.ds(0, 7 * CH)], s2)
+    all_of(resid_in.at[pl.ds(0, 15)], se)
+    all_of(mixed_in.at[pl.ds(0, 15)], sl)
+    all_of(slots_in.at[pl.ds(0, EP - 1)], s3)
+    all_of(returned.at[pl.ds(0, EP - 1)], s5)
+    all_of(stage_a, s6.at[0])
+    all_of(stage_b, s6.at[1])
+    all_of(final_a, s6f.at[0])
+    all_of(final_b, s6f.at[1])
+    all_of(core_in, s7.at[0])
+    all_of(routed_in, s7.at[1])
 
 
 def per_device(
@@ -398,6 +420,9 @@
             pltpu.VMEM((EP, CAP, WIDTH), bf16),
             pltpu.VMEM((EP, CAP, WIDTH), bf16),
             pltpu.VMEM((EP, OWN, WIDTH), bf16),
+            pltpu.VMEM((EP, OWN, MIX), bf16),
+            pltpu.VMEM((EP * OWN, WIDTH), f32),
+            pltpu.VMEM((EP * OWN, WIDTH), bf16),
             pltpu.VMEM((SLOTS, FF), bf16),
             pltpu.VMEM((EP, CAP, WIDTH), bf16),
             pltpu.VMEM((EP, CAP, WIDTH), bf16),
@@ -409,18 +434,20 @@
             pltpu.VMEM((SIDE, OWN, HALF), bf16),
             pltpu.VMEM((SIDE - 1, OWN, HALF), bf16),
             pltpu.VMEM((SIDE - 1, OWN, HALF), bf16),
-            pltpu.VMEM((TP, OWN, WIDTH), bf16),
-            pltpu.VMEM((TP, OWN, WIDTH), bf16),
+            pltpu.VMEM((SIDE, 2, OWN, WIDTH), bf16),
+            pltpu.VMEM((SIDE, OWN, WIDTH), bf16),
+            pltpu.VMEM((SIDE, OWN, WIDTH), bf16),
+            pltpu.VMEM((SIDE - 1, OWN, WIDTH), bf16),
             dma((21,)),
-            dma((TP,)), dma((TP,)),
-            dma((TP,)), dma((TP,)),
-            dma((EP,)), dma((EP,)),
-            dma((16,)), dma((16,)),
-            dma((32,)), dma((32,)),
-            dma((EP,)), dma((EP,)),
-            dma((8,)), dma((8,)),
-            dma((8,)), dma((8,)),
-            dma((TP,)), dma((TP,)),
+            dma, dma((4,)),
+            dma, dma((4,)),
+            dma, dma((8,)),
+            dma, dma((8,)),
+            dma, dma((1,)),
+            dma, dma((1,)),
+            dma((2,)), dma((2,)),
+            dma((2,)), dma((2,)),
+            dma((2,)), dma((2,)),
         ],
         compiler_params=pltpu.CompilerParams(
             collective_id=0, has_side_effects=True, vmem_limit_bytes=VMEM_MIB * 1024 * 1024

time: 58.6 us -> 54.8 us (0.935)
  Pallas kernels: 56.4 us -> 52.3 us
    pallas_call x1, Pallas kernels: 56.4 us -> 52.3 us  [per_device(): call(*[pltpu.with_memory_space_constraint(a, pltpu.HBM) for a in operands])]
where the time goes in v3:
time: 54.8 us; the launch traced here: 54.4 us
  Pallas kernels  52.3 us (95%)
  local copies, waits for them, and re-layouts  1.42 us (3%)
  between operations  0.65 us (1%)
    pallas_call x1, Pallas kernels, per_device(): call(*[pltpu.with_memory_space_constraint(a, pltpu.HBM) for a in operands])  52.3 us
    unnamed x2, local copies, waits for them, and re-layouts  1.42 us

profile of v3, /device:TPU:0, one launch (start us, length us, event | category | flops | bytes accessed | tf_op | source)
XLA Modules:
  0.0 54.4 jit_solution(8148800806685012250)
XLA Ops:
  0.6 52.3 %layer_step.1 = (bf16[16,2048]{1,0:T(8,128)(2,1)S(1)}, f32[2,128,512]{2,1,0:T(8,128)S(1)}) custom-call(bf16[128,256]{1,0:T(8,128)(2,1)} %resid_hbm.1, f32[1,2048]{1,0:T(1,128)} %bitcast.19, bf16[2048,128]{1,0:T(8,128)(2,1)} %in_w_hbm.1, f32[2,128,512]{2,1,0:T(8,128)} %state_hbm.1, f32[8,64]{1,0:T(8,128)} %decay_hbm.1, f32[8,64]{1,0:T(8,128)} %freq_hbm.1, ...), custom_call_target="tpu_custom_call" | custom-call | tf_op jit(solution)/shard_map/layer_step/pallas_call | solution.py:463
  52.9 0.6 %copy.25 = bf16[16,2048]{1,0:T(8,128)(2,1)} copy(bf16[16,2048]{1,0:T(8,128)(2,1)S(1)} %get-tuple-element.2) | data formatting | bytes 131072
  53.6 0.8 %copy.26 = f32[2,128,512]{2,1,0:T(8,128)} copy(f32[2,128,512]{2,1,0:T(8,128)S(1)} %get-tuple-element.3) | data formatting | bytes 1048576

commit v4 on v3

--- a/solution.py
+++ b/solution.py
@@ -20,7 +20,13 @@
 SLOTS = EP * CAP
 FF, SF = 512, 256
 MIX = CH * TP
+FARTHEST_FIRST = sorted(
+    [(dz, dx) for dz in range(SIDE) for dx in range(SIDE) if dz + dx],
+    key=lambda s: -min(s[0], SIDE - s[0]) - min(s[1], SIDE - s[1]),
+)
 VMEM_MIB = 48
+EARLY_COLS = 512
+EARLY_PEERS = 15
 
 
 def dot(a, b):
@@ -63,10 +69,10 @@
     resid_ref, in_gain_ref, decay_ref, freq_ref, step_ref, in_coef_ref, out_coef_ref, skip_ref,
     mid_gain_ref, gate_vec_ref, routes_ref, weights_ref,
     full, in_w, state, out_w, eg, eu, ed, sg, su, sd,
-    mixed, after, mid, outgoing, slots_in, resid_in, mixed_in, after_in, piece, hidden, result, returned,
+    own_resid, own_mixed, mixed, after, mid, outgoing, slots_in, resid_in, mixed_in, after_in, piece, hidden, result, returned,
     shidden, partial, stage_a, stage_b, sum_a, sum_b, final_a, final_b,
     routed_part, core_in, core_sum, routed_in,
-    local_sem, s1, r1, s2, r2, se, re, sl, rl, s3, r3, s5, r5, s6, r6, s6f, r6f, s7, r7,
+    local_sem, so, ro, s1, r1, s2, r2, se, re, sl, rl, s3, r3, s5, r5, s6, r6, s6f, r6f, s7, r7,
 ):
     e = lax.axis_index("ep")
     t = lax.axis_index("tp")
@@ -78,7 +84,7 @@
     ]
     ep_peers = [
         (dz * SIDE + dx, (((z + dz) % SIDE) * SIDE + (x + dx) % SIDE, t))
-        for dz in range(SIDE) for dx in range(SIDE) if dz + dx
+        for dz, dx in FARTHEST_FIRST
     ]
     x_peers = [(d, (z * SIDE + (x + d) % SIDE, t), (x + d) % SIDE) for d in (1, 3, 2)]
     z_peers = [(d, (((z + d) % SIDE) * SIDE + x, t), (z + d) % SIDE) for d in (1, 3, 2)]
@@ -125,10 +131,11 @@
 
     fetched("resid")
     cols = pl.ds(pl.multiple_of(t * FEAT, FEAT), FEAT)
-    for d, dev, _ in y_peers:
-        send(resid_ref, full.at[:, cols], s1, r1, d, dev)
-    send(resid_ref, full.at[:, cols], s1, r1, 0, partner)
+    for _, dev in tp_peers:
+        rows = pl.ds(pl.multiple_of(dev[1] * OWN, OWN), OWN)
+        send(resid_ref.at[rows], own_resid.at[:, cols], so.at[0], ro, 0, dev)
     full[:, cols] = resid_ref[...]
+    own_resid[:, cols] = resid_ref[own_rows, :]
 
     fetched("decay", "freq", "step", "in_coef", "out_coef")
     own_lane = (
@@ -176,22 +183,19 @@
     combine = jnp.where(holds, chosen_weight, 0.0).T
     comb_hi, comb_lo = halves(combine)
 
+    for d, dev, _ in y_peers:
+        send(resid_ref, full.at[:, cols], s1, r1, d, dev)
+    send(resid_ref, full.at[:, cols], s1, r1, 0, partner)
     fetched("state", "in_w", "in_gain", "skip")
     old_re, old_im = state[0], state[1]
     new_state_ref[0] = kr * old_re - ki * old_im
     new_state_ref[1] = kr * old_im + ki * old_re
-    for d in (1, 3, 2):
-        theirs = pl.ds(pl.multiple_of((((y + SIDE - d) % SIDE) * 2 + core) * FEAT, FEAT), FEAT)
-        all_of(full.at[:, theirs], r1.at[d])
-        send(full.at[:, theirs], full.at[:, theirs], s1, r1, 0, partner)
-    all_of(full.at[:, pl.ds(0, SIDE * FEAT)], r1.at[0])
-
     def first_step(src, dst, width, ss, rs):
         left, right = pl.ds(0, width), pl.ds(width, width)
         for k, (a, b) in enumerate(((left, right), (right, left))):
             for (d, dev_x, _), (_, dev_z, _) in zip(x_peers, z_peers, strict=True):
-                send(src.at[own_rows, a], dst.at[e, :, a], ss, rs, d if k == 0 else 0, dev_x)
-                send(src.at[own_rows, b], dst.at[e, :, b], ss, rs, 4 + d if k == 0 else 0, dev_z)
+                send(src.at[:, a], dst.at[e, :, a], ss, rs, d if k == 0 else 0, dev_x)
+                send(src.at[:, b], dst.at[e, :, b], ss, rs, 4 + d if k == 0 else 0, dev_z)
 
     def second_step(dst, width, ss, rs):
         left, right = pl.ds(0, width), pl.ds(width, width)
@@ -205,7 +209,15 @@
             for _, dev, _ in x_peers:
                 send(block, block, ss, rs, 0, dev)
 
-    first_step(full, resid_in, HALF, se, re)
+    all_of(own_resid.at[:, pl.ds(0, 7 * FEAT)], ro.at[0])
+    first_step(own_resid, resid_in, HALF, se, re)
+    resid_in[e] = own_resid[...]
+    for d in (1, 3, 2):
+        theirs = pl.ds(pl.multiple_of((((y + SIDE - d) % SIDE) * 2 + core) * FEAT, FEAT), FEAT)
+        all_of(full.at[:, theirs], r1.at[d])
+        send(full.at[:, theirs], full.at[:, theirs], s1, r1, 0, partner)
+    all_of(full.at[:, pl.ds(0, SIDE * FEAT)], r1.at[0])
+
     values = full[...].astype(f32)
     mean = jnp.sum(values, axis=1, keepdims=True) * (1.0 / WIDTH)
     square = jnp.sum(values * values, axis=1, keepdims=True) * (1.0 / WIDTH)
@@ -219,11 +231,16 @@
     read = dot_nt(new_re.astype(bf16), out_re) - dot_nt(new_im.astype(bf16), out_im)
     read = read + skip_ref[...] * drive.astype(f32)
     mixed_cols = pl.ds(pl.multiple_of(t * CH, CH), CH)
-    mixed[:, mixed_cols] = jax.nn.gelu(read, approximate=True).astype(bf16)
-
+    mixed_part = jax.nn.gelu(read, approximate=True).astype(bf16)
+    mixed[:, mixed_cols] = mixed_part
+
+    for _, dev in tp_peers:
+        rows = pl.ds(pl.multiple_of(dev[1] * OWN, OWN), OWN)
+        send(mixed.at[rows, mixed_cols], own_mixed.at[:, mixed_cols], so.at[1], ro, 1, dev)
+    own_mixed[:, mixed_cols] = mixed[own_rows, mixed_cols]
     for d, dev in tp_peers:
         send(mixed.at[:, mixed_cols], mixed.at[:, mixed_cols], s2, r2, d // 2, dev)
-    resid_in[e] = full[own_rows, :]
+    second_step(resid_in, HALF, se, re)
     fetched("out_w", "mid_gain")
     sums = [jnp.zeros((ROWS, 128), f32), jnp.zeros((ROWS, 128), f32)]
     for dy in (0, 1, 3, 2):
@@ -233,9 +250,6 @@
         else:
             other = pl.ds(pl.multiple_of((y * 2 + (1 - core)) * CH, CH), CH)
             all_of(mixed.at[:, other], r2.at[0])
-        if dy == 2:
-            first_step(mixed, mixed_in, MIX // 2, sl, rl)
-            mixed_in[e] = mixed[own_rows, :]
         block = mixed[:, deep]
         for j in range(WIDTH // 256):
             at = pl.ds(j * 256, 256)
@@ -247,7 +261,9 @@
                     sums[0] = sums[0] + lanes
                     sums[1] = sums[1] + lanes * lanes
         if dy == 0:
-            second_step(resid_in, HALF, se, re)
+            all_of(own_mixed.at[:, pl.ds(0, 7 * CH)], ro.at[1])
+            first_step(own_mixed, mixed_in, MIX // 2, sl, rl)
+            mixed_in[e] = own_mixed[...]
     mean = jnp.sum(sums[0], axis=1, keepdims=True) * (1.0 / WIDTH)
     square = jnp.sum(sums[1], axis=1, keepdims=True) * (1.0 / WIDTH)
     scale = lax.rsqrt(square - mean * mean + norm_eps)
@@ -257,7 +273,7 @@
         mid[:, :, at] = part.reshape(TP, OWN, 256)
         outgoing[:, :, at] = dot(pick, part).astype(bf16).reshape(EP, CAP, 256)
 
-    for d, dev in ep_peers:
+    for d, dev in ep_peers[:EARLY_PEERS]:
         send(outgoing.at[dev[0]], slots_in.at[e], s3, r3, 0, dev)
     slots_in[e] = outgoing[e]
     own_mid = mid[t]
@@ -267,6 +283,8 @@
         jnp.sum(own_mid.astype(f32) * gate_vec.astype(f32), axis=1, keepdims=True)
     )
     second_step(mixed_in, MIX // 2, sl, rl)
+    for d, dev in ep_peers[EARLY_PEERS:]:
+        send(outgoing.at[dev[0]], slots_in.at[e], s3, r3, 0, dev)
 
     fetched("eg", "eu", "ed")
     all_of(slots_in.at[pl.ds(0, EP - 1)], r3.at[0])
@@ -309,16 +327,47 @@
 
     grid = (SIDE, SIDE, OWN)
     half_a, half_b = pl.ds(0, HALF), pl.ds(HALF, HALF)
-    for half in (0, 1):
-        for j in range(HALF // 256):
-            at = pl.ds(half * HALF + j * 256, 256)
-            partial[:, :, :, at] = dot(shidden[...], sd[:, at]).astype(bf16).reshape(*grid, 256)
-        if half == 0:
-            for d, dev, there in z_peers:
-                send(partial.at[there, :, :, half_a], stage_a.at[d - 1], s6.at[0], r6, 0, dev)
-        else:
-            for d, dev, there in x_peers:
-                send(partial.at[:, there, :, half_b], stage_b.at[d - 1], s6.at[1], r6, 1, dev)
+    parts = ((0, EARLY_COLS), (EARLY_COLS, HALF - EARLY_COLS))
+
+    def partial_columns(at):
+        partial[:, :, :, at] = dot(shidden[...], sd[:, at]).astype(bf16).reshape(*grid, at.size)
+
+    def first_sums(part):
+        begin, size = parts[part]
+        at = pl.ds(begin, size)
+        left, right = at, pl.ds(HALF + begin, size)
+        for d, dev, there in z_peers:
+            send(partial.at[there, :, :, left], stage_a.at[d - 1, :, :, at], s6.at[2 * part], r6, 2 * part, dev)
+        for d, dev, there in x_peers:
+            send(partial.at[:, there, :, right], stage_b.at[d - 1, :, :, at], s6.at[2 * part + 1], r6, 2 * part + 1, dev)
+
+    def second_sums(part):
+        begin, size = parts[part]
+        at = pl.ds(begin, size)
+        left, right = at, pl.ds(HALF + begin, size)
+        all_of(stage_a.at[:, :, :, at], r6.at[2 * part])
+        total = partial[z, :, :, left].astype(f32)
+        for d in range(3):
+            total = total + stage_a[d, :, :, at].astype(f32)
+        sum_a[:, :, at] = total.astype(bf16)
+        for d, dev, there in x_peers:
+            send(sum_a.at[there, :, at], final_a.at[d - 1, :, at], s6f.at[2 * part], r6f, 2 * part, dev)
+        all_of(stage_b.at[:, :, :, at], r6.at[2 * part + 1])
+        total = partial[:, x, :, right].astype(f32)
+        for d in range(3):
+            total = total + stage_b[d, :, :, at].astype(f32)
+        sum_b[:, :, at] = total.astype(bf16)
+        for d, dev, there in z_peers:
+            send(sum_b.at[there, :, at], final_b.at[d - 1, :, at], s6f.at[2 * part + 1], r6f, 2 * part + 1, dev)
+
+    for begin in range(0, EARLY_COLS, 256):
+        partial_columns(pl.ds(begin, 256))
+        partial_columns(pl.ds(HALF + begin, 256))
+    first_sums(0)
+    for begin in range(EARLY_COLS, HALF, 256):
+        partial_columns(pl.ds(begin, 256))
+        partial_columns(pl.ds(HALF + begin, 256))
+    first_sums(1)
 
     all_of(returned.at[pl.ds(0, EP - 1)], r5.at[0])
 
@@ -333,24 +382,13 @@
     core_sum[...] = (routed_part[:, core].astype(f32) + core_in[...].astype(f32)).astype(bf16)
     for d, dev, there in y_peers:
         send(core_sum.at[there], routed_in.at[d - 1], s7.at[1], r7, 1, dev)
-    all_of(stage_a, r6.at[0])
-    total = partial[z, :, :, half_a].astype(f32)
-    for d in range(3):
-        total = total + stage_a[d].astype(f32)
-    sum_a[...] = total.astype(bf16)
-    for d, dev, there in x_peers:
-        send(sum_a.at[there], final_a.at[d - 1], s6f.at[0], r6f, 0, dev)
-    all_of(stage_b, r6.at[1])
-    total = partial[:, x, :, half_b].astype(f32)
-    for d in range(3):
-        total = total + stage_b[d].astype(f32)
-    sum_b[...] = total.astype(bf16)
-    for d, dev, there in z_peers:
-        send(sum_b.at[there], final_b.at[d - 1], s6f.at[1], r6f, 1, dev)
+    second_sums(0)
+    second_sums(1)
     all_of(routed_in, r7.at[1])
     routed = core_sum[y].astype(f32) + jnp.sum(routed_in[...].astype(f32), axis=0) + after[own_rows, :]
-    all_of(final_a, r6f.at[0])
-    all_of(final_b, r6f.at[1])
+    for part, (begin, size) in enumerate(parts):
+        all_of(final_a.at[:, :, pl.ds(begin, size)], r6f.at[2 * part])
+        all_of(final_b.at[:, :, pl.ds(begin, size)], r6f.at[2 * part + 1])
     for at, own, others in (
         (half_a, sum_a[x], final_a), (half_b, sum_b[z], final_b),
     ):
@@ -358,18 +396,33 @@
         begin = at.start
         out_ref[:, at] = (routed[:, begin : begin + HALF] + gate_value * shared).astype(bf16)
 
+    all_of(own_resid.at[:, pl.ds(0, 7 * FEAT)], so.at[0])
+    all_of(own_mixed.at[:, pl.ds(0, 7 * CH)], so.at[1])
     all_of(full.at[:, pl.ds(0, 7 * FEAT)], s1)
     all_of(mixed.at[:, pl.ds(0, 7 * CH)], s2)
     all_of(resid_in.at[pl.ds(0, 15)], se)
     all_of(mixed_in.at[pl.ds(0, 15)], sl)
     all_of(slots_in.at[pl.ds(0, EP - 1)], s3)
     all_of(returned.at[pl.ds(0, EP - 1)], s5)
-    all_of(stage_a, s6.at[0])
-    all_of(stage_b, s6.at[1])
-    all_of(final_a, s6f.at[0])
-    all_of(final_b, s6f.at[1])
+    for part, (begin, size) in enumerate(parts):
+        at = pl.ds(begin, size)
+        all_of(stage_a.at[:, :, :, at], s6.at[2 * part])
+        all_of(stage_b.at[:, :, :, at], s6.at[2 * part + 1])
+        all_of(final_a.at[:, :, at], s6f.at[2 * part])
+        all_of(final_b.at[:, :, at], s6f.at[2 * part + 1])
     all_of(core_in, s7.at[0])
     all_of(routed_in, s7.at[1])
+
+
+def write_out(out_ref, state_ref, out_hbm, state_hbm, sem):
+    copies = [
+        pltpu.make_async_copy(state_ref, state_hbm, sem.at[0]),
+        pltpu.make_async_copy(out_ref, out_hbm, sem.at[1]),
+    ]
+    for c in copies:
+        c.start()
+    for c in copies:
+        c.wait()
 
 
 def per_device(
@@ -414,6 +467,8 @@
             pltpu.VMEM((WIDTH, SF), bf16),
             pltpu.VMEM((WIDTH, SF), bf16),
             pltpu.VMEM((SF, WIDTH), bf16),
+            pltpu.VMEM((OWN, WIDTH), bf16),
+            pltpu.VMEM((OWN, MIX), bf16),
             pltpu.VMEM((ROWS, MIX), bf16),
             pltpu.VMEM((ROWS, WIDTH), f32),
             pltpu.VMEM((TP, OWN, WIDTH), bf16),
@@ -439,14 +494,15 @@
             pltpu.VMEM((SIDE, OWN, WIDTH), bf16),
             pltpu.VMEM((SIDE - 1, OWN, WIDTH), bf16),
             dma((21,)),
+            dma((2,)), dma((2,)),
             dma, dma((4,)),
             dma, dma((4,)),
             dma, dma((8,)),
             dma, dma((8,)),
             dma, dma((1,)),
             dma, dma((1,)),
-            dma((2,)), dma((2,)),
-            dma((2,)), dma((2,)),
+            dma((4,)), dma((4,)),
+            dma((4,)), dma((4,)),
             dma((2,)), dma((2,)),
         ],
         compiler_params=pltpu.CompilerParams(
@@ -460,7 +516,18 @@
         route_weight.T, expert_gate[0], expert_up[0], expert_down[0], shared_gate, shared_up,
         shared_down,
     )
-    return call(*[pltpu.with_memory_space_constraint(a, pltpu.HBM) for a in operands])
+    results = call(*[pltpu.with_memory_space_constraint(a, pltpu.HBM) for a in operands])
+    return pl.pallas_call(
+        write_out,
+        name="write_out",
+        out_shape=(
+            jax.ShapeDtypeStruct((OWN, WIDTH), bf16),
+            jax.ShapeDtypeStruct((2, ROWS, GS), f32),
+        ),
+        in_specs=[vmem, vmem],
+        out_specs=(hbm, hbm),
+        scratch_shapes=[dma((2,))],
+    )(*[pltpu.with_memory_space_constraint(a, pltpu.VMEM) for a in results])
 
 
 def solution(mesh):

time: 54.8 us -> 51.2 us (0.934)
  Pallas kernels: 52.3 us -> 50.4 us
  local copies, waits for them, and re-layouts: 1.42 us -> 0 us
    pallas_call x1, Pallas kernels: 52.3 us -> 49.6 us  [per_device(): call(*[pltpu.with_memory_space_constraint(a, pltpu.HBM) for a in operands])]
    unnamed x2 -> x0, local copies, waits for them, and re-layouts: 1.42 us -> none
    pallas_call x0 -> x1, Pallas kernels: none -> 0.82 us  [per_device(): pl.pallas_call(write_out, name='write_out', out_shape=(jax.ShapeDtypeStru...]
where the time goes in v4:
time: 51.2 us; the launch traced here: 51.1 us
  Pallas kernels  50.4 us (98%)
  between operations  0.65 us (1%)
    pallas_call x1, Pallas kernels, per_device(): call(*[pltpu.with_memory_space_constraint(a, pltpu.HBM) for a in operands])  49.6 us

profile of v4, /device:TPU:0, one launch (start us, length us, event | category | flops | bytes accessed | tf_op | source)
XLA Modules:
  0.0 51.1 jit_solution(16771933955896079251)
XLA Ops:
  0.6 49.6 %layer_step.1 = (bf16[16,2048]{1,0:T(8,128)(2,1)S(1)}, f32[2,128,512]{2,1,0:T(8,128)S(1)}) custom-call(bf16[128,256]{1,0:T(8,128)(2,1)} %resid_hbm.1, f32[1,2048]{1,0:T(1,128)} %bitcast.19, bf16[2048,128]{1,0:T(8,128)(2,1)} %in_w_hbm.1, f32[2,128,512]{2,1,0:T(8,128)} %state_hbm.1, f32[8,64]{1,0:T(8,128)} %decay_hbm.1, f32[8,64]{1,0:T(8,128)} %freq_hbm.1, ...), custom_call_target="tpu_custom_call" | custom-call | tf_op jit(solution)/shard_map/layer_step/pallas_call | solution.py:519
  50.2 0.8 %write_out.1 = (bf16[16,2048]{1,0:T(8,128)(2,1)}, f32[2,128,512]{2,1,0:T(8,128)}) custom-call(bf16[16,2048]{1,0:T(8,128)(2,1)S(1)} %get-tuple-element.4.out_ref, f32[2,128,512]{2,1,0:T(8,128)S(1)} %get-tuple-element.5.state_ref), custom_call_target="tpu_custom_call" | custom-call | tf_op jit(solution)/shard_map/write_out/pallas_call | solution.py:520

commit v5 on v4

--- a/solution.py
+++ b/solution.py
@@ -25,7 +25,8 @@
     key=lambda s: -min(s[0], SIDE - s[0]) - min(s[1], SIDE - s[1]),
 )
 VMEM_MIB = 48
-EARLY_COLS = 512
+PART = 896
+EARLY_COLS = 640
 EARLY_PEERS = 15
 
 
@@ -70,9 +71,9 @@
     mid_gain_ref, gate_vec_ref, routes_ref, weights_ref,
     full, in_w, state, out_w, eg, eu, ed, sg, su, sd,
     own_resid, own_mixed, mixed, after, mid, outgoing, slots_in, resid_in, mixed_in, after_in, piece, hidden, result, returned,
-    shidden, partial, stage_a, stage_b, sum_a, sum_b, final_a, final_b,
+    shidden, partial, stage_a, stage_b, sum_a, sum_b, final_a, final_b, direct_in,
     routed_part, core_in, core_sum, routed_in,
-    local_sem, so, ro, s1, r1, s2, r2, se, re, sl, rl, s3, r3, s5, r5, s6, r6, s6f, r6f, s7, r7,
+    local_sem, so, ro, s1, r1, s2, r2, se, re, sl, rl, s3, r3, s5, r5, s6, r6, s6d, r6d, s6f, r6f, s7, r7,
 ):
     e = lax.axis_index("ep")
     t = lax.axis_index("tp")
@@ -92,7 +93,8 @@
     partner = (e, y * 2 + (1 - core))
 
     barrier = pltpu.get_barrier_semaphore()
-    for _, dev in tp_peers + ep_peers:
+    near = [dev for _, dev in tp_peers] + [peer[1] for peer in x_peers + z_peers]
+    for dev in near:
         pl.semaphore_signal(barrier, inc=1, device_id=dev, device_id_type=MESH)
 
     fetches = {}
@@ -127,13 +129,19 @@
 
     own_rows = pl.ds(pl.multiple_of(t * OWN, OWN), OWN)
 
-    pl.semaphore_wait(barrier, TP - 1 + EP - 1)
+    pl.semaphore_wait(barrier, len(near))
 
     fetched("resid")
     cols = pl.ds(pl.multiple_of(t * FEAT, FEAT), FEAT)
     for _, dev in tp_peers:
         rows = pl.ds(pl.multiple_of(dev[1] * OWN, OWN), OWN)
         send(resid_ref.at[rows], own_resid.at[:, cols], so.at[0], ro, 0, dev)
+    for d, _, there in y_peers:
+        for c in (0, 1):
+            @pl.when(core == c)
+            def _():
+                send(resid_ref, full.at[:, cols], s1, r1, 2 * d + c, (e, there * 2 + 1))
+    send(resid_ref, full.at[:, cols], s1, r1, 0, partner)
     full[:, cols] = resid_ref[...]
     own_resid[:, cols] = resid_ref[own_rows, :]
 
@@ -183,9 +191,6 @@
     combine = jnp.where(holds, chosen_weight, 0.0).T
     comb_hi, comb_lo = halves(combine)
 
-    for d, dev, _ in y_peers:
-        send(resid_ref, full.at[:, cols], s1, r1, d, dev)
-    send(resid_ref, full.at[:, cols], s1, r1, 0, partner)
     fetched("state", "in_w", "in_gain", "skip")
     old_re, old_im = state[0], state[1]
     new_state_ref[0] = kr * old_re - ki * old_im
@@ -212,11 +217,20 @@
     all_of(own_resid.at[:, pl.ds(0, 7 * FEAT)], ro.at[0])
     first_step(own_resid, resid_in, HALF, se, re)
     resid_in[e] = own_resid[...]
-    for d in (1, 3, 2):
-        theirs = pl.ds(pl.multiple_of((((y + SIDE - d) % SIDE) * 2 + core) * FEAT, FEAT), FEAT)
-        all_of(full.at[:, theirs], r1.at[d])
-        send(full.at[:, theirs], full.at[:, theirs], s1, r1, 0, partner)
-    all_of(full.at[:, pl.ds(0, SIDE * FEAT)], r1.at[0])
+    @pl.when(core == 1)
+    def _():
+        for d in (1, 3, 2):
+            for c in (1, 0):
+                at = (((y + SIDE - d) % SIDE) * 2 + c) * FEAT
+                theirs = full.at[:, pl.ds(pl.multiple_of(at, FEAT), FEAT)]
+                all_of(theirs, r1.at[2 * d + c])
+                send(theirs, theirs, s1, r1, 0, partner)
+        all_of(full.at[:, pl.ds(0, FEAT)], r1.at[0])
+        all_of(full.at[:, pl.ds(0, 6 * FEAT)], s1)
+
+    @pl.when(core == 0)
+    def _():
+        all_of(full.at[:, pl.ds(0, 7 * FEAT)], r1.at[0])
 
     values = full[...].astype(f32)
     mean = jnp.sum(values, axis=1, keepdims=True) * (1.0 / WIDTH)
@@ -295,12 +309,19 @@
         up_part = dot(rows, eu[:, at])
         hidden[:, at] = (jax.nn.silu(gate_part) * up_part).astype(bf16)
 
+    halves_of_rows = (pl.ds(0, HALF), pl.ds(HALF, HALF))
+
+    def send_results(half):
+        at = halves_of_rows[half]
+        for _, dev in ep_peers:
+            send(result.at[dev[0], :, at], returned.at[e, :, at], s5.at[half], r5, half, dev)
+
     for j in range(WIDTH // 256):
         at = pl.ds(j * 256, 256)
         result[:, :, at] = dot(hidden[...], ed[:, at]).astype(bf16).reshape(EP, CAP, 256)
-
-    for d, dev in ep_peers:
-        send(result.at[dev[0]], returned.at[e], s5, r5, 0, dev)
+        if j == HALF // 256 - 1:
+            send_results(0)
+
     returned[e] = result[e]
 
     fetched("sg", "su", "sd")
@@ -321,21 +342,24 @@
     for j in range(WIDTH // 256):
         at = pl.ds(j * 256, 256)
         piece[:, at] = ((after_in[:, at] - mean) * scale * mid_gain_ref[:, at]).astype(bf16)
+    send_results(1)
     gate_part = dot(piece[...], sg[...])
     up_part = dot(piece[...], su[...])
     shidden[...] = (jax.nn.silu(gate_part) * up_part).astype(bf16)
 
     grid = (SIDE, SIDE, OWN)
-    half_a, half_b = pl.ds(0, HALF), pl.ds(HALF, HALF)
-    parts = ((0, EARLY_COLS), (EARLY_COLS, HALF - EARLY_COLS))
-
-    def partial_columns(at):
-        partial[:, :, :, at] = dot(shidden[...], sd[:, at]).astype(bf16).reshape(*grid, at.size)
+    direct_cols = pl.ds(2 * PART, WIDTH - 2 * PART)
+    parts = ((0, EARLY_COLS), (EARLY_COLS, PART - EARLY_COLS))
+
+    def partial_columns(first, last):
+        for begin in range(first, last, 256):
+            at = pl.ds(begin, min(256, last - begin))
+            partial[:, :, :, at] = dot(shidden[...], sd[:, at]).astype(bf16).reshape(*grid, at.size)
 
     def first_sums(part):
         begin, size = parts[part]
         at = pl.ds(begin, size)
-        left, right = at, pl.ds(HALF + begin, size)
+        left, right = at, pl.ds(PART + begin, size)
         for d, dev, there in z_peers:
             send(partial.at[there, :, :, left], stage_a.at[d - 1, :, :, at], s6.at[2 * part], r6, 2 * part, dev)
         for d, dev, there in x_peers:
@@ -344,7 +368,7 @@
     def second_sums(part):
         begin, size = parts[part]
         at = pl.ds(begin, size)
-        left, right = at, pl.ds(HALF + begin, size)
+        left, right = at, pl.ds(PART + begin, size)
         all_of(stage_a.at[:, :, :, at], r6.at[2 * part])
         total = partial[z, :, :, left].astype(f32)
         for d in range(3):
@@ -360,58 +384,68 @@
         for d, dev, there in z_peers:
             send(sum_b.at[there, :, at], final_b.at[d - 1, :, at], s6f.at[2 * part + 1], r6f, 2 * part + 1, dev)
 
-    for begin in range(0, EARLY_COLS, 256):
-        partial_columns(pl.ds(begin, 256))
-        partial_columns(pl.ds(HALF + begin, 256))
-    first_sums(0)
-    for begin in range(EARLY_COLS, HALF, 256):
-        partial_columns(pl.ds(begin, 256))
-        partial_columns(pl.ds(HALF + begin, 256))
-    first_sums(1)
-
-    all_of(returned.at[pl.ds(0, EP - 1)], r5.at[0])
-
-    for j in range(WIDTH // 256):
-        at = pl.ds(j * 256, 256)
-        back = returned[:, :, at].reshape(SLOTS, 256)
-        part = dot(comb_hi, back) + dot(comb_lo, back)
-        routed_part[:, :, :, at] = part.astype(bf16).reshape(SIDE, 2, OWN, 256)
-
-    send(routed_part.at[:, 1 - core], core_in, s7.at[0], r7, 0, partner)
-    all_of(core_in, r7.at[0])
-    core_sum[...] = (routed_part[:, core].astype(f32) + core_in[...].astype(f32)).astype(bf16)
-    for d, dev, there in y_peers:
-        send(core_sum.at[there], routed_in.at[d - 1], s7.at[1], r7, 1, dev)
+    for part, (begin, size) in enumerate(parts):
+        partial_columns(begin, begin + size)
+        partial_columns(PART + begin, PART + begin + size)
+        first_sums(part)
+    partial_columns(2 * PART, WIDTH)
+
+    for half, at in enumerate(halves_of_rows):
+        all_of(returned.at[pl.ds(0, EP - 1), :, at], r5.at[half])
+        for begin in range(0, HALF, 256):
+            part_at = pl.ds(half * HALF + begin, 256)
+            back = returned[:, :, part_at].reshape(SLOTS, 256)
+            part = dot(comb_hi, back) + dot(comb_lo, back)
+            routed_part[:, :, :, part_at] = part.astype(bf16).reshape(SIDE, 2, OWN, 256)
+        send(routed_part.at[:, 1 - core, :, at], core_in.at[:, :, at], s7.at[half], r7, half, partner)
+        all_of(core_in.at[:, :, at], r7.at[half])
+        core_sum[:, :, at] = (
+            routed_part[:, core, :, at].astype(f32) + core_in[:, :, at].astype(f32)
+        ).astype(bf16)
+        for d, dev, there in y_peers:
+            send(core_sum.at[there, :, at], routed_in.at[d - 1, :, at], s7.at[2 + half], r7, 2 + half, dev)
+    for i, (dz, dx) in enumerate(FARTHEST_FIRST):
+        to_z, to_x = (z + dz) % SIDE, (x + dx) % SIDE
+        send(
+            partial.at[to_z, to_x, :, direct_cols], direct_in.at[i], s6d, r6d, 0,
+            (to_z * SIDE + to_x, t),
+        )
     second_sums(0)
     second_sums(1)
-    all_of(routed_in, r7.at[1])
+    for half, at in enumerate(halves_of_rows):
+        all_of(routed_in.at[:, :, at], r7.at[2 + half])
     routed = core_sum[y].astype(f32) + jnp.sum(routed_in[...].astype(f32), axis=0) + after[own_rows, :]
     for part, (begin, size) in enumerate(parts):
         all_of(final_a.at[:, :, pl.ds(begin, size)], r6f.at[2 * part])
         all_of(final_b.at[:, :, pl.ds(begin, size)], r6f.at[2 * part + 1])
+    all_of(direct_in, r6d.at[0])
+    own_direct = partial[z, x, :, direct_cols]
     for at, own, others in (
-        (half_a, sum_a[x], final_a), (half_b, sum_b[z], final_b),
+        (pl.ds(0, PART), sum_a[x], final_a), (pl.ds(PART, PART), sum_b[z], final_b),
+        (direct_cols, own_direct, direct_in),
     ):
         shared = own.astype(f32) + jnp.sum(others[...].astype(f32), axis=0)
-        begin = at.start
-        out_ref[:, at] = (routed[:, begin : begin + HALF] + gate_value * shared).astype(bf16)
+        begin, size = at.start, at.size
+        out_ref[:, at] = (routed[:, begin : begin + size] + gate_value * shared).astype(bf16)
 
     all_of(own_resid.at[:, pl.ds(0, 7 * FEAT)], so.at[0])
     all_of(own_mixed.at[:, pl.ds(0, 7 * CH)], so.at[1])
-    all_of(full.at[:, pl.ds(0, 7 * FEAT)], s1)
+    all_of(full.at[:, pl.ds(0, 4 * FEAT)], s1)
     all_of(mixed.at[:, pl.ds(0, 7 * CH)], s2)
     all_of(resid_in.at[pl.ds(0, 15)], se)
     all_of(mixed_in.at[pl.ds(0, 15)], sl)
     all_of(slots_in.at[pl.ds(0, EP - 1)], s3)
-    all_of(returned.at[pl.ds(0, EP - 1)], s5)
     for part, (begin, size) in enumerate(parts):
         at = pl.ds(begin, size)
         all_of(stage_a.at[:, :, :, at], s6.at[2 * part])
         all_of(stage_b.at[:, :, :, at], s6.at[2 * part + 1])
         all_of(final_a.at[:, :, at], s6f.at[2 * part])
         all_of(final_b.at[:, :, at], s6f.at[2 * part + 1])
-    all_of(core_in, s7.at[0])
-    all_of(routed_in, s7.at[1])
+    for half, at in enumerate(halves_of_rows):
+        all_of(returned.at[pl.ds(0, EP - 1), :, at], s5.at[half])
+        all_of(core_in.at[:, :, at], s7.at[half])
+        all_of(routed_in.at[:, :, at], s7.at[2 + half])
+    all_of(direct_in, s6d)
 
 
 def write_out(out_ref, state_ref, out_hbm, state_hbm, sem):
@@ -483,27 +517,29 @@
             pltpu.VMEM((EP, CAP, WIDTH), bf16),
             pltpu.VMEM((EP * OWN, SF), bf16),
             pltpu.VMEM((SIDE, SIDE, OWN, WIDTH), bf16),
-            pltpu.VMEM((SIDE - 1, SIDE, OWN, HALF), bf16),
-            pltpu.VMEM((SIDE - 1, SIDE, OWN, HALF), bf16),
-            pltpu.VMEM((SIDE, OWN, HALF), bf16),
-            pltpu.VMEM((SIDE, OWN, HALF), bf16),
-            pltpu.VMEM((SIDE - 1, OWN, HALF), bf16),
-            pltpu.VMEM((SIDE - 1, OWN, HALF), bf16),
+            pltpu.VMEM((SIDE - 1, SIDE, OWN, PART), bf16),
+            pltpu.VMEM((SIDE - 1, SIDE, OWN, PART), bf16),
+            pltpu.VMEM((SIDE, OWN, PART), bf16),
+            pltpu.VMEM((SIDE, OWN, PART), bf16),
+            pltpu.VMEM((SIDE - 1, OWN, PART), bf16),
+            pltpu.VMEM((SIDE - 1, OWN, PART), bf16),
+            pltpu.VMEM((EP - 1, OWN, WIDTH - 2 * PART), bf16),
             pltpu.VMEM((SIDE, 2, OWN, WIDTH), bf16),
             pltpu.VMEM((SIDE, OWN, WIDTH), bf16),
             pltpu.VMEM((SIDE, OWN, WIDTH), bf16),
             pltpu.VMEM((SIDE - 1, OWN, WIDTH), bf16),
             dma((21,)),
             dma((2,)), dma((2,)),
-            dma, dma((4,)),
+            dma, dma((8,)),
             dma, dma((4,)),
             dma, dma((8,)),
             dma, dma((8,)),
             dma, dma((1,)),
+            dma((2,)), dma((2,)),
+            dma((4,)), dma((4,)),
             dma, dma((1,)),
             dma((4,)), dma((4,)),
             dma((4,)), dma((4,)),
-            dma((2,)), dma((2,)),
         ],
         compiler_params=pltpu.CompilerParams(
             collective_id=0, has_side_effects=True, vmem_limit_bytes=VMEM_MIB * 1024 * 1024

time: 51.2 us -> 49.5 us (0.967)
  Pallas kernels: 50.4 us -> 48.7 us
    pallas_call x1, Pallas kernels: 49.6 us -> 47.9 us  [per_device(): call(*[pltpu.with_memory_space_constraint(a, pltpu.HBM) for a in operands])]
where the time goes in v5:
time: 49.5 us; the launch traced here: 49.3 us
  Pallas kernels  48.7 us (98%)
  between operations  0.65 us (1%)
    pallas_call x1, Pallas kernels, per_device(): call(*[pltpu.with_memory_space_constraint(a, pltpu.HBM) for a in operands])  47.9 us

profile of v5, /device:TPU:0, one launch (start us, length us, event | category | flops | bytes accessed | tf_op | source)
XLA Modules:
  0.0 49.3 jit_solution(10142929972554438699)
XLA Ops:
  0.6 47.9 %layer_step.1 = (bf16[16,2048]{1,0:T(8,128)(2,1)S(1)}, f32[2,128,512]{2,1,0:T(8,128)S(1)}) custom-call(bf16[128,256]{1,0:T(8,128)(2,1)} %resid_hbm.1, f32[1,2048]{1,0:T(1,128)} %bitcast.19, bf16[2048,128]{1,0:T(8,128)(2,1)} %in_w_hbm.1, f32[2,128,512]{2,1,0:T(8,128)} %state_hbm.1, f32[8,64]{1,0:T(8,128)} %decay_hbm.1, f32[8,64]{1,0:T(8,128)} %freq_hbm.1, ...), custom_call_target="tpu_custom_call" | custom-call | tf_op jit(solution)/shard_map/layer_step/pallas_call | solution.py:555
  48.5 0.8 %write_out.1 = (bf16[16,2048]{1,0:T(8,128)(2,1)}, f32[2,128,512]{2,1,0:T(8,128)}) custom-call(bf16[16,2048]{1,0:T(8,128)(2,1)S(1)} %get-tuple-element.4.out_ref, f32[2,128,512]{2,1,0:T(8,128)S(1)} %get-tuple-element.5.state_ref), custom_call_target="tpu_custom_call" | custom-call | tf_op jit(solution)/shard_map/write_out/pallas_call | solution.py:556

commit v6 on v5

--- a/solution.py
+++ b/solution.py
@@ -26,6 +26,7 @@
 )
 VMEM_MIB = 48
 PART = 896
+OWN_AFTER = 3
 EARLY_COLS = 640
 EARLY_PEERS = 15
 
@@ -70,7 +71,7 @@
     resid_ref, in_gain_ref, decay_ref, freq_ref, step_ref, in_coef_ref, out_coef_ref, skip_ref,
     mid_gain_ref, gate_vec_ref, routes_ref, weights_ref,
     full, in_w, state, out_w, eg, eu, ed, sg, su, sd,
-    own_resid, own_mixed, mixed, after, mid, outgoing, slots_in, resid_in, mixed_in, after_in, piece, hidden, result, returned,
+    own_resid, own_mixed, mixed, after, outgoing, slots_in, resid_in, mixed_in, after_in, piece, hidden, result, returned,
     shidden, partial, stage_a, stage_b, sum_a, sum_b, final_a, final_b, direct_in,
     routed_part, core_in, core_sum, routed_in,
     local_sem, so, ro, s1, r1, s2, r2, se, re, sl, rl, s3, r3, s5, r5, s6, r6, s6d, r6d, s6f, r6f, s7, r7,
@@ -81,15 +82,15 @@
     y, core = t // 2, t % 2
     tp_peers = [
         (dy * 2 + dc, (e, ((y + dy) % SIDE) * 2 + (core + dc) % 2))
-        for dy in (1, 3, 2, 0) for dc in (0, 1) if dy + dc
+        for dy in (2, 1, 3, 0) for dc in (0, 1) if dy + dc
     ]
     ep_peers = [
         (dz * SIDE + dx, (((z + dz) % SIDE) * SIDE + (x + dx) % SIDE, t))
         for dz, dx in FARTHEST_FIRST
     ]
-    x_peers = [(d, (z * SIDE + (x + d) % SIDE, t), (x + d) % SIDE) for d in (1, 3, 2)]
-    z_peers = [(d, (((z + d) % SIDE) * SIDE + x, t), (z + d) % SIDE) for d in (1, 3, 2)]
-    y_peers = [(d, (e, ((y + d) % SIDE) * 2 + core), (y + d) % SIDE) for d in (1, 3, 2)]
+    x_peers = [(d, (z * SIDE + (x + d) % SIDE, t), (x + d) % SIDE) for d in (2, 1, 3)]
+    z_peers = [(d, (((z + d) % SIDE) * SIDE + x, t), (z + d) % SIDE) for d in (2, 1, 3)]
+    y_peers = [(d, (e, ((y + d) % SIDE) * 2 + core), (y + d) % SIDE) for d in (2, 1, 3)]
     partner = (e, y * 2 + (1 - core))
 
     barrier = pltpu.get_barrier_semaphore()
@@ -193,8 +194,13 @@
 
     fetched("state", "in_w", "in_gain", "skip")
     old_re, old_im = state[0], state[1]
-    new_state_ref[0] = kr * old_re - ki * old_im
-    new_state_ref[1] = kr * old_im + ki * old_re
+    kept_re = kr * old_re - ki * old_im
+    kept_im = kr * old_im + ki * old_re
+    new_state_ref[0] = kept_re
+    new_state_ref[1] = kept_im
+    read_kept = dot_nt(kept_re.astype(bf16), out_re) - dot_nt(kept_im.astype(bf16), out_im)
+    read_push = (dot_nt(pr_hi, out_re) + dot_nt(pr_lo, out_re)) - (dot_nt(pi_hi, out_im) + dot_nt(pi_lo, out_im))
+    rp_hi, rp_lo = halves(read_push)
     def first_step(src, dst, width, ss, rs):
         left, right = pl.ds(0, width), pl.ds(width, width)
         for k, (a, b) in enumerate(((left, right), (right, left))):
@@ -238,12 +244,7 @@
     scale = lax.rsqrt(square - mean * mean + norm_eps)
     normed = ((values - mean) * scale * in_gain_ref[...]).astype(bf16)
     drive = dot(normed, in_w[...]).astype(bf16)
-    new_re = new_state_ref[0] + (dot(drive, pr_hi) + dot(drive, pr_lo))
-    new_im = new_state_ref[1] + (dot(drive, pi_hi) + dot(drive, pi_lo))
-    new_state_ref[0] = new_re
-    new_state_ref[1] = new_im
-    read = dot_nt(new_re.astype(bf16), out_re) - dot_nt(new_im.astype(bf16), out_im)
-    read = read + skip_ref[...] * drive.astype(f32)
+    read = read_kept + (dot(drive, rp_hi) + dot(drive, rp_lo)) + skip_ref[...] * drive.astype(f32)
     mixed_cols = pl.ds(pl.multiple_of(t * CH, CH), CH)
     mixed_part = jax.nn.gelu(read, approximate=True).astype(bf16)
     mixed[:, mixed_cols] = mixed_part
@@ -252,8 +253,11 @@
         rows = pl.ds(pl.multiple_of(dev[1] * OWN, OWN), OWN)
         send(mixed.at[rows, mixed_cols], own_mixed.at[:, mixed_cols], so.at[1], ro, 1, dev)
     own_mixed[:, mixed_cols] = mixed[own_rows, mixed_cols]
-    for d, dev in tp_peers:
-        send(mixed.at[:, mixed_cols], mixed.at[:, mixed_cols], s2, r2, d // 2, dev)
+    for d, _, there in y_peers:
+        send(mixed.at[:, mixed_cols], mixed.at[:, mixed_cols], s2, r2, d, (e, there * 2 + 1))
+    send(mixed.at[:, mixed_cols], mixed.at[:, mixed_cols], s2, r2, 0, partner)
+    new_state_ref[0] = new_state_ref[0] + (dot(drive, pr_hi) + dot(drive, pr_lo))
+    new_state_ref[1] = new_state_ref[1] + (dot(drive, pi_hi) + dot(drive, pi_lo))
     second_step(resid_in, HALF, se, re)
     fetched("out_w", "mid_gain")
     sums = [jnp.zeros((ROWS, 128), f32), jnp.zeros((ROWS, 128), f32)]
@@ -261,6 +265,10 @@
         deep = pl.ds(pl.multiple_of(((y + SIDE - dy) % SIDE) * 256, 256), 256)
         if dy:
             all_of(mixed.at[:, deep], r2.at[dy])
+
+            @pl.when(core == 1)
+            def _():
+                send(mixed.at[:, deep], mixed.at[:, deep], s2, r2, dy, partner)
         else:
             other = pl.ds(pl.multiple_of((y * 2 + (1 - core)) * CH, CH), CH)
             all_of(mixed.at[:, other], r2.at[0])
@@ -274,7 +282,7 @@
                 for lanes in (part[:, :128], part[:, 128:]):
                     sums[0] = sums[0] + lanes
                     sums[1] = sums[1] + lanes * lanes
-        if dy == 0:
+        if dy == OWN_AFTER:
             all_of(own_mixed.at[:, pl.ds(0, 7 * CH)], ro.at[1])
             first_step(own_mixed, mixed_in, MIX // 2, sl, rl)
             mixed_in[e] = own_mixed[...]
@@ -284,13 +292,15 @@
     for j in range(WIDTH // 256):
         at = pl.ds(j * 256, 256)
         part = ((after[:, at] - mean) * scale * mid_gain_ref[:, at]).astype(bf16)
-        mid[:, :, at] = part.reshape(TP, OWN, 256)
         outgoing[:, :, at] = dot(pick, part).astype(bf16).reshape(EP, CAP, 256)
 
     for d, dev in ep_peers[:EARLY_PEERS]:
         send(outgoing.at[dev[0]], slots_in.at[e], s3, r3, 0, dev)
     slots_in[e] = outgoing[e]
-    own_mid = mid[t]
+    own_after = after[own_rows, :]
+    mean = jnp.sum(own_after, axis=1, keepdims=True) * (1.0 / WIDTH)
+    square = jnp.sum(own_after * own_after, axis=1, keepdims=True) * (1.0 / WIDTH)
+    own_mid = ((own_after - mean) * lax.rsqrt(square - mean * mean + norm_eps) * mid_gain_ref[...]).astype(bf16)
     fetched("gate_vec")
     gate_vec = jnp.concatenate([gate_vec_ref[i : i + 1, :] for i in range(WIDTH // 128)], axis=1)
     gate_value = jax.nn.sigmoid(
@@ -390,7 +400,8 @@
         first_sums(part)
     partial_columns(2 * PART, WIDTH)
 
-    for half, at in enumerate(halves_of_rows):
+    def combine_half(half):
+        at = halves_of_rows[half]
         all_of(returned.at[pl.ds(0, EP - 1), :, at], r5.at[half])
         for begin in range(0, HALF, 256):
             part_at = pl.ds(half * HALF + begin, 256)
@@ -398,19 +409,45 @@
             part = dot(comb_hi, back) + dot(comb_lo, back)
             routed_part[:, :, :, part_at] = part.astype(bf16).reshape(SIDE, 2, OWN, 256)
         send(routed_part.at[:, 1 - core, :, at], core_in.at[:, :, at], s7.at[half], r7, half, partner)
+
+    def sum_over_tp(half):
+        at = halves_of_rows[half]
         all_of(core_in.at[:, :, at], r7.at[half])
         core_sum[:, :, at] = (
             routed_part[:, core, :, at].astype(f32) + core_in[:, :, at].astype(f32)
         ).astype(bf16)
         for d, dev, there in y_peers:
             send(core_sum.at[there, :, at], routed_in.at[d - 1, :, at], s7.at[2 + half], r7, 2 + half, dev)
-    for i, (dz, dx) in enumerate(FARTHEST_FIRST):
-        to_z, to_x = (z + dz) % SIDE, (x + dx) % SIDE
-        send(
-            partial.at[to_z, to_x, :, direct_cols], direct_in.at[i], s6d, r6d, 0,
-            (to_z * SIDE + to_x, t),
-        )
-    second_sums(0)
+
+    def send_direct():
+        for i, (dz, dx) in enumerate(FARTHEST_FIRST):
+            to_z, to_x = (z + dz) % SIDE, (x + dx) % SIDE
+            send(
+                partial.at[to_z, to_x, :, direct_cols], direct_in.at[i], s6d, r6d, 0,
+                (to_z * SIDE + to_x, t),
+            )
+
+    combine_half(0)
+
+    @pl.when(core == 0)
+    def _():
+        sum_over_tp(0)
+
+    combine_half(1)
+
+    @pl.when(core == 1)
+    def _():
+        second_sums(0)
+        send_direct()
+        sum_over_tp(0)
+
+    sum_over_tp(1)
+
+    @pl.when(core == 0)
+    def _():
+        send_direct()
+        second_sums(0)
+
     second_sums(1)
     for half, at in enumerate(halves_of_rows):
         all_of(routed_in.at[:, :, at], r7.at[2 + half])
@@ -431,7 +468,12 @@
     all_of(own_resid.at[:, pl.ds(0, 7 * FEAT)], so.at[0])
     all_of(own_mixed.at[:, pl.ds(0, 7 * CH)], so.at[1])
     all_of(full.at[:, pl.ds(0, 4 * FEAT)], s1)
-    all_of(mixed.at[:, pl.ds(0, 7 * CH)], s2)
+    all_of(mixed.at[:, pl.ds(0, 4 * CH)], s2)
+
+    @pl.when(core == 1)
+    def _():
+        all_of(mixed.at[:, pl.ds(0, 6 * CH)], s2)
+
     all_of(resid_in.at[pl.ds(0, 15)], se)
     all_of(mixed_in.at[pl.ds(0, 15)], sl)
     all_of(slots_in.at[pl.ds(0, EP - 1)], s3)
@@ -505,7 +547,6 @@
             pltpu.VMEM((OWN, MIX), bf16),
             pltpu.VMEM((ROWS, MIX), bf16),
             pltpu.VMEM((ROWS, WIDTH), f32),
-            pltpu.VMEM((TP, OWN, WIDTH), bf16),
             pltpu.VMEM((EP, CAP, WIDTH), bf16),
             pltpu.VMEM((EP, CAP, WIDTH), bf16),
             pltpu.VMEM((EP, OWN, WIDTH), bf16),

time: 49.5 us -> 49 us (0.990)
  Pallas kernels: 48.7 us -> 47.8 us
    pallas_call x1, Pallas kernels: 47.9 us -> 47 us  [per_device(): call(*[pltpu.with_memory_space_constraint(a, pltpu.HBM) for a in operands])]
where the time goes in v6:
time: 49 us; the launch traced here: 48.5 us
  Pallas kernels  47.8 us (98%)
  between operations  0.65 us (1%)
    pallas_call x1, Pallas kernels, per_device(): call(*[pltpu.with_memory_space_constraint(a, pltpu.HBM) for a in operands])  47 us

profile of v6, /device:TPU:0, one launch (start us, length us, event | category | flops | bytes accessed | tf_op | source)
XLA Modules:
  0.0 48.5 jit_solution(418694918041882338)
XLA Ops:
  0.6 47.0 %layer_step.1 = (bf16[16,2048]{1,0:T(8,128)(2,1)S(1)}, f32[2,128,512]{2,1,0:T(8,128)S(1)}) custom-call(bf16[128,256]{1,0:T(8,128)(2,1)} %resid_hbm.1, f32[1,2048]{1,0:T(1,128)} %bitcast.19, bf16[2048,128]{1,0:T(8,128)(2,1)} %in_w_hbm.1, f32[2,128,512]{2,1,0:T(8,128)} %state_hbm.1, f32[8,64]{1,0:T(8,128)} %decay_hbm.1, f32[8,64]{1,0:T(8,128)} %freq_hbm.1, ...), custom_call_target="tpu_custom_call" | custom-call | tf_op jit(solution)/shard_map/layer_step/pallas_call | solution.py:596
  47.6 0.8 %write_out.1 = (bf16[16,2048]{1,0:T(8,128)(2,1)}, f32[2,128,512]{2,1,0:T(8,128)}) custom-call(bf16[16,2048]{1,0:T(8,128)(2,1)S(1)} %get-tuple-element.4.out_ref, f32[2,128,512]{2,1,0:T(8,128)S(1)} %get-tuple-element.5.state_ref), custom_call_target="tpu_custom_call" | custom-call | tf_op jit(solution)/shard_map/write_out/pallas_call | solution.py:597

commit v7 on v6

--- a/solution.py
+++ b/solution.py
@@ -20,10 +20,11 @@
 SLOTS = EP * CAP
 FF, SF = 512, 256
 MIX = CH * TP
-FARTHEST_FIRST = sorted(
-    [(dz, dx) for dz in range(SIDE) for dx in range(SIDE) if dz + dx],
-    key=lambda s: -min(s[0], SIDE - s[0]) - min(s[1], SIDE - s[1]),
+OFFSETS = (
+    [(2, 1), (2, 3), (1, 2), (3, 2), (0, 1), (0, 3), (1, 0), (3, 0)]
+    + [(2, 2), (1, 1), (1, 3), (3, 1), (3, 3), (0, 2), (2, 0)]
 )
+GROUP = EP // 2
 VMEM_MIB = 48
 PART = 896
 OWN_AFTER = 3
@@ -84,10 +85,8 @@
         (dy * 2 + dc, (e, ((y + dy) % SIDE) * 2 + (core + dc) % 2))
         for dy in (2, 1, 3, 0) for dc in (0, 1) if dy + dc
     ]
-    ep_peers = [
-        (dz * SIDE + dx, (((z + dz) % SIDE) * SIDE + (x + dx) % SIDE, t))
-        for dz, dx in FARTHEST_FIRST
-    ]
+    to_peers = [(((z + dz) % SIDE) * SIDE + (x + dx) % SIDE, t) for dz, dx in OFFSETS]
+    from_peers = [(((z + SIDE - dz) % SIDE) * SIDE + (x + SIDE - dx) % SIDE, t) for dz, dx in OFFSETS]
     x_peers = [(d, (z * SIDE + (x + d) % SIDE, t), (x + d) % SIDE) for d in (2, 1, 3)]
     z_peers = [(d, (((z + d) % SIDE) * SIDE + x, t), (z + d) % SIDE) for d in (2, 1, 3)]
     y_peers = [(d, (e, ((y + d) % SIDE) * 2 + core), (y + d) % SIDE) for d in (2, 1, 3)]
@@ -294,9 +293,12 @@
         part = ((after[:, at] - mean) * scale * mid_gain_ref[:, at]).astype(bf16)
         outgoing[:, :, at] = dot(pick, part).astype(bf16).reshape(EP, CAP, 256)
 
-    for d, dev in ep_peers[:EARLY_PEERS]:
-        send(outgoing.at[dev[0]], slots_in.at[e], s3, r3, 0, dev)
-    slots_in[e] = outgoing[e]
+    def send_slots(group):
+        for i in range(GROUP * group, min(GROUP * (group + 1), EP - 1)):
+            send(outgoing.at[to_peers[i][0]], slots_in.at[i], s3.at[group], r3, group, to_peers[i])
+
+    send_slots(0)
+    slots_in[EP - 1] = outgoing[e]
     own_after = after[own_rows, :]
     mean = jnp.sum(own_after, axis=1, keepdims=True) * (1.0 / WIDTH)
     square = jnp.sum(own_after * own_after, axis=1, keepdims=True) * (1.0 / WIDTH)
@@ -306,33 +308,36 @@
     gate_value = jax.nn.sigmoid(
         jnp.sum(own_mid.astype(f32) * gate_vec.astype(f32), axis=1, keepdims=True)
     )
+    all_of(slots_in.at[pl.ds(0, GROUP)], s3.at[0])
+    send_slots(1)
     second_step(mixed_in, MIX // 2, sl, rl)
-    for d, dev in ep_peers[EARLY_PEERS:]:
-        send(outgoing.at[dev[0]], slots_in.at[e], s3, r3, 0, dev)
 
     fetched("eg", "eu", "ed")
-    all_of(slots_in.at[pl.ds(0, EP - 1)], r3.at[0])
-    rows = slots_in[...].reshape(SLOTS, WIDTH)
-    for j in range(FF // 256):
-        at = pl.ds(j * 256, 256)
-        gate_part = dot(rows, eg[:, at])
-        up_part = dot(rows, eu[:, at])
-        hidden[:, at] = (jax.nn.silu(gate_part) * up_part).astype(bf16)
-
     halves_of_rows = (pl.ds(0, HALF), pl.ds(HALF, HALF))
 
-    def send_results(half):
-        at = halves_of_rows[half]
-        for _, dev in ep_peers:
-            send(result.at[dev[0], :, at], returned.at[e, :, at], s5.at[half], r5, half, dev)
-
-    for j in range(WIDTH // 256):
-        at = pl.ds(j * 256, 256)
-        result[:, :, at] = dot(hidden[...], ed[:, at]).astype(bf16).reshape(EP, CAP, 256)
-        if j == HALF // 256 - 1:
-            send_results(0)
-
-    returned[e] = result[e]
+    def send_results(first, last, at, k):
+        for i in range(first, last):
+            send(result.at[i, :, at], returned.at[e, :, at], s5.at[k], r5, k, from_peers[i])
+
+    for group in (0, 1):
+        number = min(GROUP, EP - 1 - GROUP * group)
+        all_of(slots_in.at[pl.ds(GROUP * group, number)], r3.at[group])
+        blocks, rows_at = pl.ds(GROUP * group, GROUP), pl.ds(GROUP * CAP * group, GROUP * CAP)
+        rows = slots_in[blocks].reshape(GROUP * CAP, WIDTH)
+        for j in range(FF // 256):
+            at = pl.ds(j * 256, 256)
+            gate_part = dot(rows, eg[:, at])
+            up_part = dot(rows, eu[:, at])
+            hidden[rows_at, at] = (jax.nn.silu(gate_part) * up_part).astype(bf16)
+        for j in range(WIDTH // 256):
+            at = pl.ds(j * 256, 256)
+            result[blocks, :, at] = dot(hidden[rows_at, :], ed[:, at]).astype(bf16).reshape(GROUP, CAP, 256)
+            if group == 1 and j == HALF // 256 - 1:
+                send_results(GROUP, EP - 1, halves_of_rows[0], 1)
+        if group == 0:
+            send_results(0, GROUP, pl.ds(0, WIDTH), 0)
+
+    returned[e] = result[EP - 1]
 
     fetched("sg", "su", "sd")
     all_of(resid_in.at[pl.ds(0, 12)], re.at[0])
@@ -352,7 +357,7 @@
     for j in range(WIDTH // 256):
         at = pl.ds(j * 256, 256)
         piece[:, at] = ((after_in[:, at] - mean) * scale * mid_gain_ref[:, at]).astype(bf16)
-    send_results(1)
+    send_results(GROUP, EP - 1, halves_of_rows[1], 2)
     gate_part = dot(piece[...], sg[...])
     up_part = dot(piece[...], su[...])
     shidden[...] = (jax.nn.silu(gate_part) * up_part).astype(bf16)
@@ -402,7 +407,9 @@
 
     def combine_half(half):
         at = halves_of_rows[half]
-        all_of(returned.at[pl.ds(0, EP - 1), :, at], r5.at[half])
+        if half == 0:
+            all_of(returned.at[pl.ds(0, GROUP)], r5.at[0])
+        all_of(returned.at[pl.ds(0, EP - 1 - GROUP), :, at], r5.at[1 + half])
         for begin in range(0, HALF, 256):
             part_at = pl.ds(half * HALF + begin, 256)
             back = returned[:, :, part_at].reshape(SLOTS, 256)
@@ -420,7 +427,7 @@
             send(core_sum.at[there, :, at], routed_in.at[d - 1, :, at], s7.at[2 + half], r7, 2 + half, dev)
 
     def send_direct():
-        for i, (dz, dx) in enumerate(FARTHEST_FIRST):
+        for i, (dz, dx) in enumerate(OFFSETS):
             to_z, to_x = (z + dz) % SIDE, (x + dx) % SIDE
             send(
                 partial.at[to_z, to_x, :, direct_cols], direct_in.at[i], s6d, r6d, 0,
@@ -476,7 +483,8 @@
 
     all_of(resid_in.at[pl.ds(0, 15)], se)
     all_of(mixed_in.at[pl.ds(0, 15)], sl)
-    all_of(slots_in.at[pl.ds(0, EP - 1)], s3)
+    all_of(slots_in.at[pl.ds(0, EP - 1 - GROUP)], s3.at[1])
+    all_of(returned.at[pl.ds(0, GROUP)], s5.at[0])
     for part, (begin, size) in enumerate(parts):
         at = pl.ds(begin, size)
         all_of(stage_a.at[:, :, :, at], s6.at[2 * part])
@@ -484,7 +492,7 @@
         all_of(final_a.at[:, :, at], s6f.at[2 * part])
         all_of(final_b.at[:, :, at], s6f.at[2 * part + 1])
     for half, at in enumerate(halves_of_rows):
-        all_of(returned.at[pl.ds(0, EP - 1), :, at], s5.at[half])
+        all_of(returned.at[pl.ds(0, EP - 1 - GROUP), :, at], s5.at[1 + half])
         all_of(core_in.at[:, :, at], s7.at[half])
         all_of(routed_in.at[:, :, at], s7.at[2 + half])
     all_of(direct_in, s6d)
@@ -575,8 +583,8 @@
             dma, dma((4,)),
             dma, dma((8,)),
             dma, dma((8,)),
-            dma, dma((1,)),
             dma((2,)), dma((2,)),
+            dma((3,)), dma((3,)),
             dma((4,)), dma((4,)),
             dma, dma((1,)),
             dma((4,)), dma((4,)),

time: 49 us -> 48.4 us (0.988)
  no operation moved by 1% of the time
where the time goes in v7:
time: 48.4 us; the launch traced here: 48.2 us
  Pallas kernels  47.6 us (98%)
  between operations  0.65 us (1%)
    pallas_call x1, Pallas kernels, per_device(): call(*[pltpu.with_memory_space_constraint(a, pltpu.HBM) for a in operands])  46.8 us

profile of v7, /device:TPU:0, one launch (start us, length us, event | category | flops | bytes accessed | tf_op | source)
XLA Modules:
  0.0 48.2 jit_solution(1497168267845615845)
XLA Ops:
  0.6 46.8 %layer_step.1 = (bf16[16,2048]{1,0:T(8,128)(2,1)S(1)}, f32[2,128,512]{2,1,0:T(8,128)S(1)}) custom-call(bf16[128,256]{1,0:T(8,128)(2,1)} %resid_hbm.1, f32[1,2048]{1,0:T(1,128)} %bitcast.19, bf16[2048,128]{1,0:T(8,128)(2,1)} %in_w_hbm.1, f32[2,128,512]{2,1,0:T(8,128)} %state_hbm.1, f32[8,64]{1,0:T(8,128)} %decay_hbm.1, f32[8,64]{1,0:T(8,128)} %freq_hbm.1, ...), custom_call_target="tpu_custom_call" | custom-call | tf_op jit(solution)/shard_map/layer_step/pallas_call | solution.py:604
  47.4 0.8 %write_out.1 = (bf16[16,2048]{1,0:T(8,128)(2,1)}, f32[2,128,512]{2,1,0:T(8,128)}) custom-call(bf16[16,2048]{1,0:T(8,128)(2,1)S(1)} %get-tuple-element.4.out_ref, f32[2,128,512]{2,1,0:T(8,128)S(1)} %get-tuple-element.5.state_ref), custom_call_target="tpu_custom_call" | custom-call | tf_op jit(solution)/shard_map/write_out/pallas_call | solution.py:605

commit v8 on v7

--- a/solution.py
+++ b/solution.py
@@ -29,7 +29,6 @@
 PART = 896
 OWN_AFTER = 3
 EARLY_COLS = 640
-EARLY_PEERS = 15
 
 
 def dot(a, b):
@@ -376,9 +375,9 @@
         at = pl.ds(begin, size)
         left, right = at, pl.ds(PART + begin, size)
         for d, dev, there in z_peers:
-            send(partial.at[there, :, :, left], stage_a.at[d - 1, :, :, at], s6.at[2 * part], r6, 2 * part, dev)
+            send(partial.at[there, :, :, left], stage_a.at[d - 1, :, :, at], s6.at[0], r6, 2 * part, dev)
         for d, dev, there in x_peers:
-            send(partial.at[:, there, :, right], stage_b.at[d - 1, :, :, at], s6.at[2 * part + 1], r6, 2 * part + 1, dev)
+            send(partial.at[:, there, :, right], stage_b.at[d - 1, :, :, at], s6.at[1], r6, 2 * part + 1, dev)
 
     def second_sums(part):
         begin, size = parts[part]
@@ -390,14 +389,14 @@
             total = total + stage_a[d, :, :, at].astype(f32)
         sum_a[:, :, at] = total.astype(bf16)
         for d, dev, there in x_peers:
-            send(sum_a.at[there, :, at], final_a.at[d - 1, :, at], s6f.at[2 * part], r6f, 2 * part, dev)
+            send(sum_a.at[there, :, at], final_a.at[d - 1, :, at], s6f.at[0], r6f, 0, dev)
         all_of(stage_b.at[:, :, :, at], r6.at[2 * part + 1])
         total = partial[:, x, :, right].astype(f32)
         for d in range(3):
             total = total + stage_b[d, :, :, at].astype(f32)
         sum_b[:, :, at] = total.astype(bf16)
         for d, dev, there in z_peers:
-            send(sum_b.at[there, :, at], final_b.at[d - 1, :, at], s6f.at[2 * part + 1], r6f, 2 * part + 1, dev)
+            send(sum_b.at[there, :, at], final_b.at[d - 1, :, at], s6f.at[1], r6f, 1, dev)
 
     for part, (begin, size) in enumerate(parts):
         partial_columns(begin, begin + size)
@@ -415,7 +414,7 @@
             back = returned[:, :, part_at].reshape(SLOTS, 256)
             part = dot(comb_hi, back) + dot(comb_lo, back)
             routed_part[:, :, :, part_at] = part.astype(bf16).reshape(SIDE, 2, OWN, 256)
-        send(routed_part.at[:, 1 - core, :, at], core_in.at[:, :, at], s7.at[half], r7, half, partner)
+        send(routed_part.at[:, 1 - core, :, at], core_in.at[:, :, at], s7.at[0], r7, half, partner)
 
     def sum_over_tp(half):
         at = halves_of_rows[half]
@@ -424,7 +423,7 @@
             routed_part[:, core, :, at].astype(f32) + core_in[:, :, at].astype(f32)
         ).astype(bf16)
         for d, dev, there in y_peers:
-            send(core_sum.at[there, :, at], routed_in.at[d - 1, :, at], s7.at[2 + half], r7, 2 + half, dev)
+            send(core_sum.at[there, :, at], routed_in.at[d - 1, :, at], s7.at[1], r7, 2, dev)
 
     def send_direct():
         for i, (dz, dx) in enumerate(OFFSETS):
@@ -456,12 +455,10 @@
         second_sums(0)
 
     second_sums(1)
-    for half, at in enumerate(halves_of_rows):
-        all_of(routed_in.at[:, :, at], r7.at[2 + half])
+    all_of(routed_in, r7.at[2])
     routed = core_sum[y].astype(f32) + jnp.sum(routed_in[...].astype(f32), axis=0) + after[own_rows, :]
-    for part, (begin, size) in enumerate(parts):
-        all_of(final_a.at[:, :, pl.ds(begin, size)], r6f.at[2 * part])
-        all_of(final_b.at[:, :, pl.ds(begin, size)], r6f.at[2 * part + 1])
+    all_of(final_a, r6f.at[0])
+    all_of(final_b, r6f.at[1])
     all_of(direct_in, r6d.at[0])
     own_direct = partial[z, x, :, direct_cols]
     for at, own, others in (
@@ -485,17 +482,15 @@
     all_of(mixed_in.at[pl.ds(0, 15)], sl)
     all_of(slots_in.at[pl.ds(0, EP - 1 - GROUP)], s3.at[1])
     all_of(returned.at[pl.ds(0, GROUP)], s5.at[0])
-    for part, (begin, size) in enumerate(parts):
-        at = pl.ds(begin, size)
-        all_of(stage_a.at[:, :, :, at], s6.at[2 * part])
-        all_of(stage_b.at[:, :, :, at], s6.at[2 * part + 1])
-        all_of(final_a.at[:, :, at], s6f.at[2 * part])
-        all_of(final_b.at[:, :, at], s6f.at[2 * part + 1])
+    all_of(stage_a, s6.at[0])
+    all_of(stage_b, s6.at[1])
+    all_of(final_a, s6f.at[0])
+    all_of(final_b, s6f.at[1])
     for half, at in enumerate(halves_of_rows):
         all_of(returned.at[pl.ds(0, EP - 1 - GROUP), :, at], s5.at[1 + half])
-        all_of(core_in.at[:, :, at], s7.at[half])
-        all_of(routed_in.at[:, :, at], s7.at[2 + half])
     all_of(direct_in, s6d)
+    all_of(core_in, s7.at[0])
+    all_of(routed_in, s7.at[1])
 
 
 def write_out(out_ref, state_ref, out_hbm, state_hbm, sem):
@@ -585,10 +580,10 @@
             dma, dma((8,)),
             dma((2,)), dma((2,)),
             dma((3,)), dma((3,)),
-            dma((4,)), dma((4,)),
+            dma((2,)), dma((4,)),
             dma, dma((1,)),
-            dma((4,)), dma((4,)),
-            dma((4,)), dma((4,)),
+            dma((2,)), dma((2,)),
+            dma((2,)), dma((3,)),
         ],
         compiler_params=pltpu.CompilerParams(
             collective_id=0, has_side_effects=True, vmem_limit_bytes=VMEM_MIB * 1024 * 1024

time: 48.4 us -> 48.3 us (level)
  no operation moved by 1% of the time
where the time goes in v8:
time: 48.3 us; the launch traced here: 48.2 us
  Pallas kernels  47.5 us (98%)
  between operations  0.65 us (1%)
    pallas_call x1, Pallas kernels, per_device(): call(*[pltpu.with_memory_space_constraint(a, pltpu.HBM) for a in operands])  46.7 us

profile of v8, /device:TPU:0, one launch (start us, length us, event | category | flops | bytes accessed | tf_op | source)
XLA Modules:
  0.0 48.2 jit_solution(10670682991658489836)
XLA Ops:
  0.6 46.7 %layer_step.1 = (bf16[16,2048]{1,0:T(8,128)(2,1)S(1)}, f32[2,128,512]{2,1,0:T(8,128)S(1)}) custom-call(bf16[128,256]{1,0:T(8,128)(2,1)} %resid_hbm.1, f32[1,2048]{1,0:T(1,128)} %bitcast.19, bf16[2048,128]{1,0:T(8,128)(2,1)} %in_w_hbm.1, f32[2,128,512]{2,1,0:T(8,128)} %state_hbm.1, f32[8,64]{1,0:T(8,128)} %decay_hbm.1, f32[8,64]{1,0:T(8,128)} %freq_hbm.1, ...), custom_call_target="tpu_custom_call" | custom-call | tf_op jit(solution)/shard_map/layer_step/pallas_call | solution.py:599
  47.3 0.8 %write_out.1 = (bf16[16,2048]{1,0:T(8,128)(2,1)}, f32[2,128,512]{2,1,0:T(8,128)}) custom-call(bf16[16,2048]{1,0:T(8,128)(2,1)S(1)} %get-tuple-element.4.out_ref, f32[2,128,512]{2,1,0:T(8,128)S(1)} %get-tuple-element.5.state_ref), custom_call_target="tpu_custom_call" | custom-call | tf_op jit(solution)/shard_map/write_out/pallas_call | solution.py:600
